TPU v7x, 128 devices: a whole 4x4x4 slice. The times are simulated.
128 devices in a mesh: sp: 32 (over z, y, core), tp: 4 (over x).
Axes of the slice: x: 4, y: 4, z: 4, core: 2. Of those that a mesh axis runs over, the one named last changes fastest.
Arguments:
- tokens: bfloat16 [32768, 2048], P(('sp', 'tp')), may hold values from -6 to 6
- norm_gain: float32 [2048], replicated, may hold values from 0.1 to 1.9
- w_query: bfloat16 [2048, 2048], P(None, 'tp'), may hold values from -0.125 to 0.125
- w_forget: bfloat16 [2048, 2048], P(None, 'tp'), may hold values from -0.125 to 0.125
- w_value: bfloat16 [2048, 2048], P(None, 'tp'), may hold values from -0.125 to 0.125
- w_rgate: bfloat16 [2048, 2048], P(None, 'tp'), may hold values from -0.125 to 0.125
- w_glu_value: bfloat16 [2048, 2048], P(None, 'tp'), may hold values from -0.125 to 0.125
- w_glu_gate: bfloat16 [2048, 2048], P(None, 'tp'), may hold values from -0.125 to 0.125
- forget_gap: float32 [2048], P('tp'), may hold values from 1.5258789e-05 to 0.1
- decay_shift: float32 [32768, 16], P('sp', 'tp'), may hold values from -0.6 to 0, as said below
- head_gain: float32 [128], replicated, may hold values from 0.1 to 1.9
- conv_taps: float32 [31, 2048], P(None, 'tp'), may hold values from -12 to 12
- conv_gain: float32 [2048], P('tp'), may hold values from 0.1 to 1.9
- out_rec: bfloat16 [2048, 2048], P('tp'), may hold values from -0.09375 to 0.09375
- out_conv: bfloat16 [2048, 2048], P('tp'), may hold values from -0.09375 to 0.09375
Outputs:
- mixed: bfloat16 [32768, 2048], P(('sp', 'tp'))
Inputs may be any that keep to these rules, and one draw needn't show every extreme that they name: `decay_shift`: at most zero everywhere.
All inputs are finite; a program needn't handle non-finite values.
Results may differ from a plain program's by a relative error of at most 0.015.
Values may be sent and summed in bfloat16 or wider, within the bound.
A program may use at most 128 MiB of HBM per device.

v0:
```python
import jax
import jax.numpy as jnp
from jax import lax
from jax.sharding import PartitionSpec as P

HEAD = 128
BLOCK = 64


norm_epsilon = 1e-05
head_epsilon = 1e-06


def from_everyone(array, axis):
    copies = jnp.broadcast_to(array, (lax.axis_size(axis), *array.shape))
    return lax.all_to_all(copies, axis, split_axis=0, concat_axis=0, tiled=True)


def in_order(blocks, dim):
    shape = list(blocks.shape[1:])
    shape[dim] *= blocks.shape[0]
    return jnp.moveaxis(blocks, 0, dim).reshape(shape)


def gathered_copies(array, axis, dim):
    blocks = from_everyone(array, axis)
    return in_order(blocks, dim)


def from_behind(value, axis, steps):
    count = lax.axis_size(axis)
    first, last = (max(0, -steps), min(count, count - steps))
    return lax.ppermute(value, axis, [(source, source + steps) for source in range(first, last)])


def work_in_pieces(array, axis, dim, apply, out_dim):
    size, extent = (lax.axis_size(axis), array.shape[dim])
    count = 2 if extent % 2 == 0 else 1
    finished, length = ([], extent // count)
    for k in range(count):
        share = lax.slice_in_dim(array, k * length, (k + 1) * length, axis=dim)
        starts = jnp.arange(size) * extent + k * length
        finished.append(jax.vmap(apply)(lax.all_gather(share, axis), starts))
    return in_order(jnp.concatenate(finished, axis=out_dim + 1), out_dim)


def layer_norm(values, gain):
    widened = values.astype(jnp.float32)
    row_mean = jnp.mean(widened, axis=-1, keepdims=True)
    centred = widened - row_mean
    row_var = jnp.mean(centred * centred, axis=-1, keepdims=True)
    return centred * lax.rsqrt(row_var + norm_epsilon) * gain


def local_scan(query, key_gate, values, log_forget):
    row_count, head_count, key_width = query.shape
    value_width = values.shape[2]
    block_count = row_count // BLOCK

    def to_blocks(array):
        return array.reshape(block_count, BLOCK, head_count, array.shape[2]).transpose(0, 2, 1, 3)

    def from_blocks(array):
        return array.transpose(0, 2, 1, 3).reshape(row_count, head_count, array.shape[3])

    causal = lax.broadcasted_iota(jnp.int32, (BLOCK, BLOCK), 0) >= lax.broadcasted_iota(
        jnp.int32, (BLOCK, BLOCK), 1
    )

    def advance(carried, inputs):
        current_state, offset = carried
        query_blk, key_block, value_block, log_blk = inputs
        running_total = jnp.cumsum(log_blk, axis=1)
        closing_log = running_total[:, -1:, :]
        query_decayed = query_blk * jnp.exp(running_total)
        scores = jnp.einsum("htk,hsk->hts", query_decayed, key_block * jnp.exp(-running_total))
        scores = jnp.where(causal[None], scores, 0.0)
        output_rows = jnp.einsum("hts,hsv->htv", scores, value_block)
        output_rows = output_rows + jnp.einsum("ori,oiq->orq", query_decayed, current_state)
        query_distant = query_blk * jnp.exp(running_total + offset[:, None, :])
        current_state = jnp.exp(closing_log[:, 0, :])[:, :, None] * current_state + jnp.einsum(
            "itp,ito->ipo", key_block * jnp.exp(closing_log - running_total), value_block
        )
        return ((current_state, offset + closing_log[:, 0, :]), (output_rows, query_distant))

    start_state = jnp.zeros((head_count, key_width, value_width), jnp.float32)
    start_offset = jnp.zeros((head_count, key_width), jnp.float32)
    final, stacked = lax.scan(
        advance,
        (start_state, start_offset),
        (to_blocks(query), to_blocks(key_gate), to_blocks(values), to_blocks(log_forget)),
    )
    return (final[0], final[1], from_blocks(stacked[0]), from_blocks(stacked[1]))


def recur(query_raw, forget_raw, value_raw, rgate_raw, forget_gap, decay_shift, head_gain):
    row_count = query_raw.shape[0]
    head_count = query_raw.shape[1] // HEAD
    query = jax.nn.silu(query_raw.astype(jnp.float32)).reshape(row_count, head_count, HEAD)
    key_gate = forget_gap * jax.nn.sigmoid(-forget_raw.astype(jnp.float32))
    log_forget = jnp.log1p(-key_gate).reshape(row_count, head_count, HEAD) + decay_shift[:, :, None]
    values = value_raw.astype(jnp.float32).reshape(row_count, head_count, HEAD)
    final_state, total_log, nearby_output, query_distant = local_scan(
        query, key_gate.reshape(row_count, head_count, HEAD), values, log_forget
    )
    logs_all = gathered_copies(total_log[None], "sp", 0)
    after_logs = jnp.cumsum(logs_all, axis=0)
    my_index = lax.axis_index("sp")
    own_log = lax.dynamic_index_in_dim(after_logs - logs_all, my_index, 0, keepdims=False)
    segment_piece = lax.all_gather(
        final_state[None].astype(jnp.bfloat16), "sp", axis=0, tiled=True
    ).astype(jnp.float32)
    piece_rows = segment_piece.shape[0]
    indices = jnp.arange(piece_rows, dtype=jnp.int32)
    multiplier = jnp.where(
        (indices < my_index)[:, None, None],
        jnp.exp(jnp.minimum(own_log[None] - after_logs, 0.0)),
        0.0,
    )
    arriving_state = jnp.zeros_like(final_state) + jnp.einsum(
        "dbq,dbqu->bqu", multiplier, segment_piece
    )
    recurrent_branch = nearby_output + jnp.einsum("bji,jiy->bjy", query_distant, arriving_state)
    recurrent_branch = (
        recurrent_branch
        * lax.rsqrt(
            jnp.mean(recurrent_branch * recurrent_branch, axis=-1, keepdims=True) + head_epsilon
        )
        * head_gain
    )
    return (
        recurrent_branch.reshape(row_count, head_count * HEAD)
        * jax.nn.silu(rgate_raw.astype(jnp.float32))
    ).astype(jnp.bfloat16)


def convolve(glu_value, glu_gate, conv_taps, conv_gain):
    row_count = glu_value.shape[0]
    mixed_in = (
        glu_value.astype(jnp.float32) * jax.nn.sigmoid(glu_gate.astype(jnp.float32))
    ).astype(jnp.bfloat16)
    reach = conv_taps.shape[0] - 1
    rim = from_behind(mixed_in[row_count - reach :], "sp", 1)
    padded = lax.optimization_barrier(jnp.concatenate([rim, mixed_in], axis=0)).astype(jnp.float32)
    filtered = jnp.zeros(glu_value.shape, jnp.float32)
    for tap_index in range(reach + 1):
        filtered = filtered + conv_taps[tap_index] * padded[tap_index : tap_index + row_count]
    row_sum, row_square = lax.psum(
        (jnp.sum(filtered, axis=1), jnp.sum(filtered * filtered, axis=1)), "tp"
    )
    channels = filtered.shape[1] * lax.axis_size("tp")
    row_mean = row_sum / channels
    row_var = row_square / channels - row_mean * row_mean
    normed = (filtered - row_mean[:, None]) * lax.rsqrt(row_var[:, None] + norm_epsilon) * conv_gain
    return jax.nn.silu(normed).astype(jnp.bfloat16)


def on_device(
    tokens,
    norm_gain,
    w_query,
    w_forget,
    w_value,
    w_rgate,
    w_glu_value,
    w_glu_gate,
    forget_gap,
    decay_shift,
    head_gain,
    conv_taps,
    conv_gain,
    out_rec,
    out_conv,
):
    weights = (w_query, w_forget, w_value, w_rgate, w_glu_value, w_glu_gate)

    def project(segment_piece, first_row):
        normed = layer_norm(segment_piece, norm_gain).astype(jnp.bfloat16)
        return jnp.concatenate(
            [
                jnp.dot(normed, weight, preferred_element_type=jnp.float32).astype(jnp.bfloat16)
                for weight in weights
            ],
            axis=1,
        )

    projected_in = work_in_pieces(tokens, "tp", 0, project, 0)
    rec_width = w_query.shape[1]
    conv_width = w_glu_value.shape[1]
    query_raw = projected_in[:, 0:rec_width]
    forget_raw = projected_in[:, rec_width : 2 * rec_width]
    value_raw = projected_in[:, 2 * rec_width : 3 * rec_width]
    rgate_raw = projected_in[:, 3 * rec_width : 4 * rec_width]
    glu_value = projected_in[:, 4 * rec_width : 4 * rec_width + conv_width]
    glu_gate = projected_in[:, 4 * rec_width + conv_width : 4 * rec_width + 2 * conv_width]
    conv_out = convolve(glu_value, glu_gate, conv_taps, conv_gain)
    rec_out = recur(query_raw, forget_raw, value_raw, rgate_raw, forget_gap, decay_shift, head_gain)
    return lax.psum_scatter(
        (
            jnp.dot(rec_out, out_rec, preferred_element_type=jnp.float32)
            + jnp.dot(conv_out, out_conv, preferred_element_type=jnp.float32)
        ).astype(jnp.bfloat16),
        "tp",
        scatter_dimension=0,
        tiled=True,
    )


def solution(mesh):
    placed = (
        P(("sp", "tp"), None),
        P(),
        P(None, "tp"),
        P(None, "tp"),
        P(None, "tp"),
        P(None, "tp"),
        P(None, "tp"),
        P(None, "tp"),
        P("tp"),
        P("sp", "tp"),
        P(),
        P(None, "tp"),
        P("tp"),
        P("tp", None),
        P("tp", None),
    )
    return jax.shard_map(
        on_device, mesh=mesh, in_specs=placed, out_specs=P(("sp", "tp"), None), check_vma=False
    )
```

profile of v0, /device:TPU:0, one launch (start us, length us, event | category | flops | bytes accessed | tf_op | source)
XLA Modules:
  0.0 319.2 jit_solution(3020927366686600964)
XLA Ops:
  6.5 2.5 fusion.174
  11.0 31.5 %all-gather.7.cloned.1.call-done = bf16[512,2048]{1,0:T(8,128)(2,1)} async-done(((bf16[128,2048]{1,0:T(8,128)(2,1)}), bf16[512,2048]{1,0:T(8,128)(2,1)}) %all-gather.7.cloned.1.call-update) | async-done | bytes 2097168 | tf_op jit(solution)/shard_map/all_gather | solution.py:43
  42.5 2.3 convert_element_type.114
  45.7 29.3 %all-gather.9.cloned.1.call-done = bf16[512,2048]{1,0:T(8,128)(2,1)} async-done(((bf16[128,2048]{1,0:T(8,128)(2,1)}), bf16[512,2048]{1,0:T(8,128)(2,1)}) %all-gather.9.cloned.1.call-update) | async-done | bytes 2097168 | tf_op jit(solution)/shard_map/all_gather | solution.py:43
  82.0 2.1 fusion.89
  88.8 2.1 fusion.113
  92.2 2.1 fusion.125
  95.6 2.1 fusion.137
  99.0 2.1 fusion.149
  101.1 2.3 pad_maximum_fusion
  104.6 3.7 %multiply_convert_fusion.3 = (bf16[1024,512]{1,0:T(8,128)(2,1)S(1)}, f32[1024,512]{1,0:T(8,128)}, f32[1024,512]{1,0:T(8,128)}, f32[1024,512]{1,0:T(8,128)}) fusion(bf16[1024,3072]{1,0:T(8,128)(2,1)S(1)} %bitcast.220, f32[512]{0:T(512)S(1)} %copy-done.11), kind=kLoop, calls=%fused_computation.141 | loop fusion | flops 8912896 | bytes 11536384 | tf_op jit(solution)/shard_map/convert_element_type | solution.py:141
  110.2 3.2 reshape_reshape.10
  113.4 2.1 reshape.91
  115.5 2.9 reshape_reshape.12
  118.4 3.2 add_bitcast_fusion
  121.6 80.5 %while.17 = (s32[]{:T(128)}, f32[4,128,128]{2,1,0:T(8,128)S(1)}, f32[4,128]{1,0:T(4,128)S(1)}, f32[16,4,64,128]{3,2,0,1:T(8,128)}, bf16[16,4,64,128]{3,2,0,1:T(8...) while((s32[]{:T(128)}, f32[4,128,128]{2,1,0:T(8,128)S(1)}, ...), condition=%wide.region_6.0_spmd.clone, body=%wide.region_4.6_spmd.clone.sunk | while | flops 27808772 | bytes 4092065 | solution.py:88
  207.1 8.5 %all-to-all-start = ((f32[32,1,4,128]{3,2,1,0:T(4,128)}), f32[32,1,4,128]{3,2,1,0:T(4,128)S(1)}, u32[]{:S(2)}, u32[]{:S(2)}) async-start(f32[32,1,4,128]{3,2,1,0:T(4,128)} %broadcast_in_dim.35), calls=%async_computation | async-start | bytes 131072 | tf_op jit(solution)/shard_map/all_to_all | solution.py:16
  216.2 9.5 %fusion.171 = (f32[1024]{0:T(1024)S(1)}, f32[1024]{0:T(1024)S(1)}, f32[1024,512]{1,0:T(8,128)}) fusion(f32[1054,512]{1,0:T(8,128)S(1)} %convert_element_type.111, f32[512]{0:T(512)S(1)} %bitcast.246, f32[512]{0:T(512)S(1)} %bitcast.247, f32[512]{0:T(512)S(1)} %bitcast.249, f32[512]{0:T(512)S(1)} %bitcast.250, f32[512]{0:T(512)S(1)} %bitcast.251, ...), kind=kLoop, calls=%fused_computation.198 | loop fusion | flops 33552384 | bytes 67180544 | tf_op jit(solution)/shard_map/reduce_sum | solution.py:149
  225.7 8.7 %all-reduce = (f32[1024]{0:T(1024)S(1)}, f32[1024]{0:T(1024)S(1)}) all-reduce(f32[1024]{0:T(1024)S(1)} %get-tuple-element.115, f32[1024]{0:T(1024)S(1)} %get-tuple-element.114), channel_id=1, replica_groups=mesh['sp'=32,'tp'=4] {'tp'}, use_global_device_ids=true, to_apply=%region_12.13 | all-reduce | flops 2048 | bytes 16384 | tf_op jit(solution)/shard_map/psum | solution.py:148
  234.5 14.7 %all-gather.11.cloned.1.call-done = bf16[128,128,128]{2,1,0:T(8,128)(2,1)} async-done(((bf16[4,128,128]{2,1,0:T(8,128)(2,1)}), bf16[128,128,128]{2,1,0:T(8,128)(2,1)}) %all-gather.11.cloned.1.call-update) | async-done | bytes 4194320 | tf_op jit(solution)/shard_map/all_gather | solution.py:110
  249.2 4.5 %multiply_reduce_fusion = bf16[4,128,128]{2,1,0:T(8,128)(2,1)S(1)} fusion(bf16[4,128,32,128]{3,1,0,2:T(8,128)(2,1)} %bitcast.226, f32[4,128,32]{1,0,2:T(4,128)S(1)} %select_bitcast_fusion), kind=kLoop, calls=%fused_computation.35 | loop fusion | flops 6225920 | bytes 4390912 | tf_op jit(solution)/shard_map/dbq,dbqu->bqu/dot_general | solution.py:120
  256.7 5.1 %fusion.158 = f32[1024,2048]{1,0:T(8,128)S(1)} fusion(bf16[512,2048]{1,0:T(8,128)(2,1)} %param.30, f32[1024,512]{1,0:T(8,128)} %copy.36, bf16[1024,3072]{1,0:T(8,128)(2,1)} %bitcast.221), kind=kOutput, calls=%fused_computation.173 | convolution fusion | flops 2151153664 | bytes 13631488 | tf_op jit(solution)/shard_map/dot_general | solution.py:200
  261.8 4.6 %add_convert_fusion = bf16[1024,2048]{1,0:T(8,128)(2,1)} fusion(f32[1024,2048]{1,0:T(8,128)S(1)} %fusion.158, bf16[512,2048]{1,0:T(8,128)(2,1)S(1)} %copy-done.18, f32[1024,512]{1,0:T(8,128)S(1)} %copy-done.6, f32[512]{0:T(512)S(1)} %copy-done.19, f32[1024]{0:T(1024)S(1)} %get-tuple-element.184, f32[1024]{0:T(1024)S(1)} %get-tuple-element.183), kind=kOutput, calls=%fused_computation.36 | convolution fusion | flops 2155872256 | bytes 16787456 | tf_op jit(solution)/shard_map/dot_general | solution.py:201
  266.4 46.2 %reduce-scatter.2.cloned.1.call-done = bf16[256,2048]{1,0:T(8,128)(2,1)} async-done(((bf16[1024,2048]{1,0:T(8,128)(2,1)}), bf16[256,2048]{1,0:T(8,128)(2,1)}) %reduce-scatter.2.cloned.1.call-update) | async-done | bytes 1048592 | tf_op jit(solution)/shard_map/reduce_scatter | solution.py:198
  (284 shorter events, 109.8 us)
Async XLA Ops:
  6.5 74.2 %copy-start = (bf16[2048,512]{1,0:T(8,128)(2,1)S(1)}, bf16[2048,512]{1,0:T(8,128)(2,1)}, u32[]{:S(2)}) copy-start(bf16[2048,512]{1,0:T(8,128)(2,1)} %param.19) | copy-start | bytes 6291460
  6.5 3.4 %copy-start.9 = (f32[1024,4]{0,1:T(4,128)S(1)}, f32[1024,4]{0,1:T(4,128)}, u32[]{:S(2)}) copy-start(f32[1024,4]{0,1:T(4,128)} %param.26) | copy-start | bytes 49156
  6.5 35.9 %all-gather.7.cloned.1.call-start = ((), (), s32[]{:S(2)}) async-start(), calls=%async_computation.3 | async-start | bytes 2621440 | tf_op jit(solution)/shard_map/all_gather | solution.py:43
  9.1 65.9 %all-gather.9.cloned.1.call-start = ((), (), s32[]{:S(2)}) async-start(), calls=%async_computation.4 | async-start | bytes 2621440 | tf_op jit(solution)/shard_map/all_gather | solution.py:43
  9.8 239.4 %all-gather.11.cloned.1.call-start = ((), (), s32[]{:S(2)}) async-start(), calls=%async_computation.5 | async-start | bytes 4325376 | tf_op jit(solution)/shard_map/all_gather | solution.py:110
  42.5 2.3 copy-start.3
  74.9 2.2 copy-start.5
  77.7 1.6 copy-start.4
  77.7 1.6 copy-start.10
  82.0 2.1 copy-start.13
  85.4 2.1 copy-start.14
  88.8 2.2 copy-start.15
  92.2 2.1 copy-start.16
  95.6 2.1 copy-start.17
  103.4 4.8 %copy-start.2 = (bf16[4,256,3072]{2,1,0:T(8,128)(2,1)}, bf16[4,256,3072]{2,1,0:T(8,128)(2,1)S(1)}, u32[]{:S(2)}) copy-start(bf16[4,256,3072]{2,1,0:T(8,128)(2,1)S(1)} %pad_maximum_fusion) | copy-start | bytes 18874372
  121.6 81.2 %copy-start.8 = (f32[31,512]{1,0:T(8,128)S(1)}, f32[31,512]{1,0:T(8,128)}, u32[]{:S(2)}) copy-start(f32[31,512]{1,0:T(8,128)} %param.28) | copy-start | bytes 190468
  202.9 12.7 %collective-permute-start = (bf16[30,512]{1,0:T(8,128)(2,1)S(1)}, bf16[30,512]{1,0:T(8,128)(2,1)S(1)}, u32[]{:S(2)}, u32[]{:S(2)}) collective-permute-start(bf16[30,512]{1,0:T(8,128)(2,1)S(1)} %slice.295), channel_id=1, source_target_pairs={{0,4},{4,8},{8,12},{12,16},{16,20},{20,24},{24,28},{28,32},{32,36}... | collective-permute-start | bytes 92168 | tf_op jit(solution)/shard_map/ppermute | solution.py:33
  207.1 27.3 %all-to-all-start = ((f32[32,1,4,128]{3,2,1,0:T(4,128)}), f32[32,1,4,128]{3,2,1,0:T(4,128)S(1)}, u32[]{:S(2)}, u32[]{:S(2)}) async-start(f32[32,1,4,128]{3,2,1,0:T(4,128)} %broadcast_in_dim.35), calls=%async_computation | async-start | bytes 131072 | tf_op jit(solution)/shard_map/all_to_all | solution.py:16
  215.6 97.0 %reduce-scatter.2.cloned.1.call-start = ((), (), s32[]{:S(2)}) async-start(), calls=%async_computation.2 | async-start | bytes 5242880 | tf_op jit(solution)/shard_map/reduce_scatter | solution.py:198
  249.2 4.5 %copy-start.7 = (bf16[16,4,64,128]{3,2,0,1:T(8,128)(2,1)S(1)}, bf16[16,4,64,128]{3,2,0,1:T(8,128)(2,1)}, u32[]{:S(2)}) copy-start(bf16[16,4,64,128]{3,2,0,1:T(8,128)(2,1)} %get-tuple-element.63) | copy-start | bytes 3145732
  256.7 5.1 %copy-start.6 = (f32[1024,512]{1,0:T(8,128)S(1)}, f32[1024,512]{1,0:T(8,128)}, u32[]{:S(2)}) copy-start(f32[1024,512]{1,0:T(8,128)} %get-tuple-element.138) | copy-start | bytes 6291460
  256.7 5.1 %copy-start.18 = (bf16[512,2048]{1,0:T(8,128)(2,1)S(1)}, bf16[512,2048]{1,0:T(8,128)(2,1)}, u32[]{:S(2)}) copy-start(bf16[512,2048]{1,0:T(8,128)(2,1)} %param.31) | copy-start | bytes 6291460
  256.7 5.1 %copy-start.19 = (f32[512]{0:T(512)S(1)}, f32[512]{0:T(512)}, u32[]{:S(2)}) copy-start(f32[512]{0:T(512)} %param.29) | copy-start | bytes 6148
  266.4 46.2 %copy-start.1 = (bf16[2048,512]{1,0:T(8,128)(2,1)S(1)}, bf16[2048,512]{1,0:T(8,128)(2,1)}, u32[]{:S(2)}) copy-start(bf16[2048,512]{1,0:T(8,128)(2,1)} %param.19) | copy-start | bytes 6291460
  (2 other events, 1.8 us)
Sparse Core Ops, SparseCore 0:
  9.2 33.2 all-gather.6
  44.1 30.7 all-gather.8
  202.9 46.2 all-gather.10
  266.5 46.0 reduce-scatter.1
where the time goes:
time: 322 us; the launch traced here: 319 us
  waiting for transfers between devices  122 us (38%)
  local copies, waits for them, and re-layouts  65.3 us (20%)
  matrix products  52.6 us (16%)
  other arithmetic  46 us (14%)
  between operations  13.6 us (4%)
  starting transfers between devices  10.2 us (3%)
  blocking collectives  8.68 us (3%)
    all_gather x2, waiting for transfers between devices, work_in_pieces(): finished.append(jax.vmap(apply)(lax.all_gather(share, axis), starts))  60.8 us
    reduce_scatter x1, waiting for transfers between devices, on_device(): lax.psum_scatter((jnp.dot(rec_out, out_rec, preferred_element_type=jnp.fl...  46.2 us
    dynamic_slice x64, local copies, waits for them, and re-layouts, local_scan(): lax.scan(advance, (start_state, start_offset), (to_blocks(query), to_bloc...  44.5 us
    dot_general x12, matrix products, project(): jnp.dot(normed, weight, preferred_element_type=jnp.float32)  20.2 us
    all_gather x1, waiting for transfers between devices, recur(): lax.all_gather(final_state[None].astype(jnp.bfloat16), 'sp', axis=0, tile...  14.7 us
    dot_general x16, matrix products, advance(): jnp.einsum('ori,oiq->orq', query_decayed, current_state)  13.1 us
    dynamic_update_slice x16, other arithmetic, local_scan(): lax.scan(advance, (start_state, start_offset), (to_blocks(query), to_bloc...  10.6 us
    reduce_sum x1, other arithmetic, convolve(): jnp.sum(filtered, axis=1)  9.47 us
  transfers between devices with their start and end apart: 6, of which 4 were waited for; matrix products, arithmetic and copies ran while one was open for 5% of the time, Pallas kernels for 0%

commit v1 on v0

v1 whole, which is shorter than its diff:
```python
import jax
import jax.numpy as jnp
from jax import lax
from jax.experimental import pallas as pl
from jax.experimental.pallas import tpu as pltpu
from jax.sharding import PartitionSpec as P

MESH = pl.DeviceIdType.MESH
HEAD = 128
UNIT = 128
f32 = jnp.float32
bf16 = jnp.bfloat16

norm_epsilon = 1e-05
head_epsilon = 1e-06

NT = (((1,), (1,)), ((), ()))
TN = (((0,), (0,)), ((), ()))


def dot(a, b):
    return jnp.dot(a, b, preferred_element_type=f32)


def split3(value):
    hi = value.astype(bf16)
    rest = value - hi.astype(f32)
    mid = rest.astype(bf16)
    low = (rest - mid.astype(f32)).astype(bf16)
    return hi, mid, low


def pack_state(state, log):
    hi, mid, low = split3(log)
    row = lax.broadcasted_iota(jnp.int32, (16, state.shape[1]), 0)
    extra = jnp.where(
        row == 0,
        hi.astype(f32),
        jnp.where(row == 1, mid.astype(f32), jnp.where(row == 2, low.astype(f32), 0.0)),
    )
    return state.astype(bf16), extra.astype(bf16)


def unpack_state(ref):
    state = ref[0:128, :].astype(f32)
    log = jnp.sum(ref[128:144, :].astype(f32), axis=0, keepdims=True)
    return state, log


def kernel(
    tokens,
    norm_gain,
    w_query,
    w_forget,
    w_value,
    w_rgate,
    w_glu_value,
    w_glu_gate,
    gap,
    shift,
    head_gain,
    taps,
    conv_gain,
    out_rec,
    out_conv,
    out,
    tok,
    xn,
    xp,
    w_in,
    w_out,
    raw,
    hml,
    run,
    keys,
    kdec,
    near,
    qfar,
    rgate,
    pad,
    filt,
    s_unit,
    a_unit,
    h_unit,
    s_loc,
    a_loc,
    p_send,
    p_recv,
    y_msg,
    z_msg,
    h_in,
    stat,
    o_in,
    part,
    s_buf,
    r_buf,
    load_sem,
    ag_send,
    ag_recv,
    sp_send,
    sp_recv,
    st_send,
    st_recv,
    rs_send,
    rs_recv,
):
    x = lax.axis_index("tp")
    s = lax.axis_index("sp")
    core = lax.rem(s, 2)
    chip = s // 2
    y = lax.rem(chip, 4)
    z = chip // 4
    right = lax.rem(x + 1, 4)
    left = lax.rem(x + 3, 4)
    far = lax.rem(x + 2, 4)
    behind = lax.rem(s + 31, 32)
    ahead = lax.rem(s + 1, 32)
    partner = chip * 2 + (1 - core)

    def at_y(k):
        return (z * 4 + lax.rem(y + k, 4)) * 2 + core

    def at_z(k):
        return (lax.rem(z + k, 4) * 4 + y) * 2 + core

    barrier = pltpu.get_barrier_semaphore()
    peers = [{"tp": right}, {"tp": left}, {"tp": far}, {"sp": partner}, {"sp": behind}]
    peers += [{"sp": at_y(k)} for k in (1, 2, 3)] + [{"sp": at_z(k)} for k in (1, 2, 3)]
    for peer in peers:
        pl.semaphore_signal(barrier, inc=1, device_id=peer, device_id_type=MESH)

    loads = [
        pltpu.make_async_copy(tokens, tok, load_sem.at[0]),
    ]
    for k, weight in enumerate((w_forget, w_value, w_query, w_rgate, w_glu_value, w_glu_gate)):
        loads.append(pltpu.make_async_copy(weight, w_in.at[k], load_sem.at[1 + k]))
    loads.append(pltpu.make_async_copy(out_rec, w_out.at[pl.ds(0, 512)], load_sem.at[7]))
    loads.append(pltpu.make_async_copy(out_conv, w_out.at[pl.ds(512, 512)], load_sem.at[8]))
    for load in loads:
        load.start()

    def norm_rows(piece):
        @pl.loop(0, UNIT // 16)
        def _(i):
            row = pl.multiple_of(i * 16, 16)
            wide = tok[pl.ds(piece * UNIT + row, 16), :].astype(f32)
            mean = jnp.mean(wide, axis=1, keepdims=True)
            centred = wide - mean
            var = jnp.mean(centred * centred, axis=1, keepdims=True)
            value = centred * lax.rsqrt(var + norm_epsilon) * norm_gain[...]
            xn[2 * x + piece, pl.ds(row, 16), :] = value.astype(bf16)

    def send_unit(unit, k, target):
        return pltpu.make_async_remote_copy(
            src_ref=xn.at[unit],
            dst_ref=xn.at[unit],
            send_sem=ag_send.at[k],
            recv_sem=ag_recv.at[k],
            device_id={"tp": target},
            device_id_type=MESH,
        )

    gather = [
        send_unit(2 * x, 0, right),
        send_unit(2 * x + 1, 1, right),
        send_unit(2 * left, 2, right),
        send_unit(2 * x + 1, 3, left),
        send_unit(2 * x, 4, left),
        send_unit(2 * right + 1, 5, left),
    ]
    arrive = [
        send_unit(2 * left, 0, right),
        send_unit(2 * left + 1, 1, right),
        send_unit(2 * far, 2, right),
        send_unit(2 * right + 1, 3, left),
        send_unit(2 * right, 4, left),
        send_unit(2 * far + 1, 5, left),
    ]
    loads[0].wait()
    norm_rows(0)
    pl.semaphore_wait(barrier, len(peers))
    gather[0].start()
    norm_rows(1)
    gather[3].start()
    gather[1].start()
    gather[4].start()

    keep = lax.broadcasted_iota(jnp.int32, (UNIT, UNIT), 0) >= lax.broadcasted_iota(
        jnp.int32, (UNIT, UNIT), 1
    )
    ones_low = jnp.where(keep, 1.0, 0.0).astype(bf16)
    tri = jnp.concatenate([ones_low, ones_low, ones_low], axis=1)

    def lanes(h):
        return slice(h * HEAD, (h + 1) * HEAD)

    def sp_copy(src, dst, k, target):
        return pltpu.make_async_remote_copy(
            src_ref=src,
            dst_ref=dst,
            send_sem=sp_send.at[k],
            recv_sem=sp_recv.at[k],
            device_id={"sp": target},
            device_id_type=MESH,
        )

    def pair_copy():
        return sp_copy(p_send, p_recv, 0, partner)

    @pl.loop(0, 4)
    def _(step):
        unit_a = jnp.where(
            step == 0,
            2 * x,
            jnp.where(step == 1, 2 * left, jnp.where(step == 2, 2 * left + 1, 2 * far)),
        )
        unit_b = jnp.where(
            step == 0,
            2 * x + 1,
            jnp.where(step == 1, 2 * right + 1, jnp.where(step == 2, 2 * right, 2 * far + 1)),
        )

        @pl.when(step == 0)
        def _():
            for k in range(1, 7):
                loads[k].wait()

        @pl.when(step == 1)
        def _():
            arrive[0].wait_recv()
            gather[2].start()
            arrive[3].wait_recv()
            gather[5].start()

        @pl.when(step == 2)
        def _():
            arrive[1].wait_recv()
            arrive[4].wait_recv()

        @pl.when(step == 3)
        def _():
            arrive[2].wait_recv()
            arrive[5].wait_recv()

        xp[0:UNIT, :] = xn[unit_a]
        xp[UNIT : 2 * UNIT, :] = xn[unit_b]
        for k in (0, 1):
            raw[k] = dot(xp[...], w_in[k]).astype(bf16)

        @pl.loop(0, 2)
        def _(k):
            unit = jnp.where(k == 0, unit_a, unit_b)
            row = pl.multiple_of(k * UNIT, UNIT)
            rows = pl.ds(row, UNIT)
            for h in range(4):
                forget = raw[0, rows, lanes(h)].astype(f32)
                gate = gap[:, lanes(h)] * jax.nn.sigmoid(-forget)
                in_unit = pl.ds(pl.multiple_of(unit * UNIT, UNIT), UNIT)
                log = jnp.log1p(-gate) + shift[in_unit, h : h + 1]
                hi, mid, low = split3(log)
                hml[0:UNIT, lanes(h)] = hi
                hml[UNIT : 2 * UNIT, lanes(h)] = mid
                hml[2 * UNIT : 3 * UNIT, lanes(h)] = low
                keys[:, lanes(h)] = gate
            total = dot(tri, hml[...])
            run[k] = total
            a_unit[unit] = jnp.broadcast_to(total[UNIT - 1 : UNIT, :], (8, 512))
            for h in range(4):
                run_h = run[k, :, lanes(h)]
                centre = run_h[63:64, :]
                end = run_h[127:128, :]
                decayed = keys[:, lanes(h)] * jnp.exp(centre - run_h)
                kdec[k, :, lanes(h)] = decayed.astype(bf16)
                ending = (decayed * jnp.exp(end - centre)).astype(bf16)
                s_unit[unit, :, lanes(h)] = lax.dot_general(
                    raw[1, rows, lanes(h)], ending, TN, preferred_element_type=f32
                )

        @pl.when(step == 3)
        def _():
            state = s_unit[0]
            log = a_unit[0, 0:1, :]
            for u in range(1, 8):
                a_u = a_unit[u, 0:1, :]
                state = state * jnp.exp(a_u) + s_unit[u]
                log = log + a_u
            for half in range(2):
                part_of = slice(half * 256, half * 256 + 256)
                s_loc[half] = state[:, part_of]
                a_loc[half] = jnp.broadcast_to(log[:, part_of], (8, 256))
            body, extra = pack_state(s_loc[1 - core], a_loc[1 - core, 0:1, :])
            p_send[0:128, :] = body
            p_send[128:144, :] = extra
            pair_copy().start()

        for k in (2, 3, 4, 5):
            raw[k] = dot(xp[...], w_in[k]).astype(bf16)

        @pl.loop(0, 2)
        def _(k):
            unit = jnp.where(k == 0, unit_a, unit_b)
            row = pl.multiple_of(k * UNIT, UNIT)
            rows = pl.ds(row, UNIT)
            for h in range(4):
                run_h = run[k, :, lanes(h)]
                centre = run_h[63:64, :]
                query = raw[2, rows, lanes(h)].astype(f32)
                query = query * jax.nn.sigmoid(query) * jnp.exp(run_h - centre)
                qfar[unit, :, lanes(h)] = (query * jnp.exp(centre)).astype(bf16)
                scores = lax.dot_general(
                    query.astype(bf16), kdec[k, :, lanes(h)], NT, preferred_element_type=f32
                )
                scores = jnp.where(keep, scores, 0.0).astype(bf16)
                near[unit, :, lanes(h)] = dot(scores, raw[1, rows, lanes(h)])
                rgate[unit, :, lanes(h)] = raw[3, rows, lanes(h)]
                value = raw[4, rows, lanes(h)].astype(f32)
                mixed = value * jax.nn.sigmoid(raw[5, rows, lanes(h)].astype(f32))
                pad[h, pl.ds(pl.multiple_of(32 + unit * UNIT, 32), UNIT), :] = mixed.astype(
                    bf16
                ).astype(f32)

    edge = sp_copy(pad.at[:, pl.ds(1024, 32), :], pad.at[:, pl.ds(0, 32), :], 1, ahead)
    along_y = [sp_copy(y_msg.at[y], y_msg.at[y], 1 + k, at_y(k)) for k in (1, 2, 3)]
    along_z = [sp_copy(z_msg.at[z], z_msg.at[z], 4 + k, at_z(k)) for k in (1, 2, 3)]
    swap = sp_copy(h_in.at[1 - core, core], h_in.at[1 - core, core], 8, partner)

    edge.start()

    pair_copy().wait()
    mine, mine_log = s_loc[core], a_loc[core, 0:1, :]
    other, other_log = unpack_state(p_recv)
    first = jnp.where(core == 0, mine, other)
    first_log = jnp.where(core == 0, mine_log, other_log)
    second = jnp.where(core == 0, other, mine)
    second_log = jnp.where(core == 0, other_log, mine_log)
    s_loc[core] = first
    a_loc[core] = jnp.broadcast_to(first_log, (8, 256))
    body, extra = pack_state(first * jnp.exp(second_log) + second, first_log + second_log)
    y_msg[y, 0:128, :] = body
    y_msg[y, 128:144, :] = extra
    for copy in along_y:
        copy.start()

    def filter_unit(unit):
        start = unit * UNIT + 2
        lane = lax.broadcasted_iota(jnp.int32, (UNIT, HEAD), 1)
        sums = jnp.zeros((UNIT, 1), f32)
        squares = jnp.zeros((UNIT, 1), f32)
        for g in range(4):
            total = jnp.zeros((UNIT, HEAD), f32)
            for j in range(31):
                total = total + taps[j : j + 1, lanes(g)] * pad[g, pl.ds(start + j, UNIT), :]
            filt[unit, :, lanes(g)] = total
            sums = sums + jnp.sum(total, axis=1, keepdims=True)
            squares = squares + jnp.sum(total * total, axis=1, keepdims=True)
        old = stat[0]
        stat[0] = jnp.where(lane == unit, sums, jnp.where(lane == unit + 8, squares, old))

    stat[0] = jnp.zeros((UNIT, HEAD), f32)

    @pl.loop(1, 5)
    def _(unit):
        filter_unit(unit)

    for copy in along_y:
        copy.wait()
    whole = jnp.zeros((128, 256), f32)
    whole_log = jnp.zeros((1, 256), f32)
    before = jnp.zeros((128, 256), f32)
    before_log = jnp.zeros((1, 256), f32)
    for k in range(4):
        state, log = unpack_state(y_msg.at[k])
        before = jnp.where(k == y, whole, before)
        before_log = jnp.where(k == y, whole_log, before_log)
        whole = whole * jnp.exp(log) + state
        whole_log = whole_log + log
    body, extra = pack_state(whole, whole_log)
    z_msg[z, 0:128, :] = body
    z_msg[z, 128:144, :] = extra
    for copy in along_z:
        copy.start()
    y_before, y_before_log = before, before_log
    s_loc[1 - core] = y_before
    a_loc[1 - core] = jnp.broadcast_to(y_before_log, (8, 256))

    @pl.loop(5, 8)
    def _(unit):
        filter_unit(unit)

    edge.wait()

    @pl.when(s == 0)
    def _():
        pad[:, 0:32, :] = jnp.zeros((4, 32, HEAD), f32)

    filter_unit(0)

    def stat_copy(k):
        return pltpu.make_async_remote_copy(
            src_ref=stat.at[0],
            dst_ref=stat.at[k],
            send_sem=st_send.at[k],
            recv_sem=st_recv.at[k],
            device_id={"tp": lax.rem(x + k, 4)},
            device_id_type=MESH,
        )

    stats = [stat_copy(k) for k in (1, 2, 3)]
    for copy in stats:
        copy.start()

    for copy in along_z:
        copy.wait()
    whole = jnp.zeros((128, 256), f32)
    before = jnp.zeros((128, 256), f32)
    for k in range(4):
        state, log = unpack_state(z_msg.at[k])
        before = jnp.where(k == z, whole, before)
        whole = whole * jnp.exp(log) + state
    chip_in = before * jnp.exp(a_loc[1 - core, 0:1, :]) + s_loc[1 - core]
    h_in[0, core] = chip_in
    h_in[1, core] = chip_in * jnp.exp(a_loc[core, 0:1, :]) + s_loc[core]
    swap.start()
    for copy in stats:
        copy.wait()
    stat[0] = (stat[0] + stat[1]) + (stat[2] + stat[3])
    loads[7].wait()
    loads[8].wait()
    swap.wait()

    state = jnp.concatenate([h_in[core, 0], h_in[core, 1]], axis=1)
    for u in range(8):
        h_unit[u] = state.astype(bf16)
        if u < 7:
            state = state * jnp.exp(a_unit[u, 0:1, :]) + s_unit[u]

    def scatter(k, target):
        return pltpu.make_async_remote_copy(
            src_ref=s_buf.at[k],
            dst_ref=r_buf.at[k],
            send_sem=rs_send.at[k],
            recv_sem=rs_recv.at[k],
            device_id={"tp": target},
            device_id_type=MESH,
        )

    reduce = [scatter(k, left if k in (0, 3, 4) else right) for k in range(6)]

    @pl.loop(0, 4)
    def _(step):
        unit_a = jnp.where(
            step == 0,
            2 * far,
            jnp.where(step == 1, 2 * right, jnp.where(step == 2, 2 * left, 2 * x)),
        )
        unit_b = jnp.where(
            step == 0,
            2 * far + 1,
            jnp.where(step == 1, 2 * left + 1, jnp.where(step == 2, 2 * right + 1, 2 * x + 1)),
        )

        @pl.loop(0, 2)
        def _(k):
            unit = jnp.where(k == 0, unit_a, unit_b)
            rows = pl.ds(pl.multiple_of(k * UNIT, UNIT), UNIT)
            lane = lax.broadcasted_iota(jnp.int32, (UNIT, HEAD), 1)
            totals = stat[0]
            sums = jnp.sum(jnp.where(lane == unit, totals, 0.0), axis=1, keepdims=True)
            squares = jnp.sum(jnp.where(lane == unit + 8, totals, 0.0), axis=1, keepdims=True)
            mean = sums * (1.0 / 2048)
            scale = lax.rsqrt(squares * (1.0 / 2048) - mean * mean + norm_epsilon)
            for h in range(4):
                rec = near[unit, :, lanes(h)] + lax.dot_general(
                    qfar[unit, :, lanes(h)],
                    h_unit[unit, :, lanes(h)],
                    NT,
                    preferred_element_type=f32,
                )
                power = jnp.mean(rec * rec, axis=1, keepdims=True)
                gate = rgate[unit, :, lanes(h)].astype(f32)
                rec = rec * lax.rsqrt(power + head_epsilon) * head_gain[...]
                o_in[rows, lanes(h)] = (rec * (gate * jax.nn.sigmoid(gate))).astype(bf16)
                conv = (filt[unit, :, lanes(h)] - mean) * scale * conv_gain[:, lanes(h)]
                o_in[rows, lanes(4 + h)] = (conv * jax.nn.sigmoid(conv)).astype(bf16)

        for c in range(4):
            cols = slice(c * 512, c * 512 + 512)
            part[:, cols] = dot(o_in[...], w_out[:, cols])

        for i in (0, 1):

            @pl.when(step == i)
            def _(i=i):
                s_buf[2 * i] = part[0:UNIT, :].astype(bf16)
                reduce[2 * i].start()
                s_buf[2 * i + 1] = part[UNIT : 2 * UNIT, :].astype(bf16)
                reduce[2 * i + 1].start()

        @pl.when(step == 2)
        def _():
            reduce[0].wait_recv()
            s_buf[4] = (part[0:UNIT, :] + r_buf[0].astype(f32)).astype(bf16)
            reduce[4].start()
            reduce[1].wait_recv()
            s_buf[5] = (part[UNIT : 2 * UNIT, :] + r_buf[1].astype(f32)).astype(bf16)
            reduce[5].start()

    for k in (2, 3, 4, 5):
        reduce[k].wait_recv()
    out[0:UNIT, :] = (
        part[0:UNIT, :] + r_buf[2].astype(f32) + r_buf[4].astype(f32)
    ).astype(bf16)
    out[UNIT : 2 * UNIT, :] = (
        part[UNIT : 2 * UNIT, :] + r_buf[3].astype(f32) + r_buf[5].astype(f32)
    ).astype(bf16)
    for copy in gather:
        copy.wait_send()
    for copy in reduce:
        copy.wait_send()


def on_device(
    tokens,
    norm_gain,
    w_query,
    w_forget,
    w_value,
    w_rgate,
    w_glu_value,
    w_glu_gate,
    forget_gap,
    decay_shift,
    head_gain,
    conv_taps,
    conv_gain,
    out_rec,
    out_conv,
):
    vmem = pl.BlockSpec(memory_space=pltpu.VMEM)
    hbm = pl.BlockSpec(memory_space=pl.ANY)
    dma = pltpu.SemaphoreType.DMA
    scratch = [
        pltpu.VMEM((256, 2048), bf16),
        pltpu.VMEM((8, 128, 2048), bf16),
        pltpu.VMEM((256, 2048), bf16),
        pltpu.VMEM((6, 2048, 512), bf16),
        pltpu.VMEM((1024, 2048), bf16),
        pltpu.VMEM((6, 256, 512), bf16),
        pltpu.VMEM((384, 512), bf16),
        pltpu.VMEM((2, 128, 512), f32),
        pltpu.VMEM((128, 512), f32),
        pltpu.VMEM((2, 128, 512), bf16),
        pltpu.VMEM((8, 128, 512), f32),
        pltpu.VMEM((8, 128, 512), bf16),
        pltpu.VMEM((8, 128, 512), bf16),
        pltpu.VMEM((4, 1056, 128), f32),
        pltpu.VMEM((8, 128, 512), f32),
        pltpu.VMEM((8, 128, 512), f32),
        pltpu.VMEM((8, 8, 512), f32),
        pltpu.VMEM((8, 128, 512), bf16),
        pltpu.VMEM((2, 128, 256), f32),
        pltpu.VMEM((2, 8, 256), f32),
        pltpu.VMEM((144, 256), bf16),
        pltpu.VMEM((144, 256), bf16),
        pltpu.VMEM((4, 144, 256), bf16),
        pltpu.VMEM((4, 144, 256), bf16),
        pltpu.VMEM((2, 2, 128, 256), f32),
        pltpu.VMEM((4, 128, 128), f32),
        pltpu.VMEM((256, 1024), bf16),
        pltpu.VMEM((256, 2048), f32),
        pltpu.VMEM((6, 128, 2048), bf16),
        pltpu.VMEM((6, 128, 2048), bf16),
        dma((9,)),
        dma((6,)),
        dma((6,)),
        dma((9,)),
        dma((9,)),
        dma((4,)),
        dma((4,)),
        dma((6,)),
        dma((6,)),
    ]
    return pl.pallas_call(
        kernel,
        out_shape=jax.ShapeDtypeStruct((256, 2048), bf16),
        in_specs=[hbm, vmem] + [hbm] * 6 + [vmem] * 5 + [hbm] * 2,
        out_specs=vmem,
        scratch_shapes=scratch,
        compiler_params=pltpu.CompilerParams(
            collective_id=0, has_side_effects=True, vmem_limit_bytes=62 * 1024 * 1024
        ),
    )(
        tokens,
        norm_gain[None],
        w_query,
        w_forget,
        w_value,
        w_rgate,
        w_glu_value,
        w_glu_gate,
        forget_gap[None],
        decay_shift,
        head_gain[None],
        conv_taps,
        conv_gain[None],
        out_rec,
        out_conv,
    )


def solution(mesh):
    placed = (
        P(("sp", "tp"), None),
        P(),
        P(None, "tp"),
        P(None, "tp"),
        P(None, "tp"),
        P(None, "tp"),
        P(None, "tp"),
        P(None, "tp"),
        P("tp"),
        P("sp", "tp"),
        P(),
        P(None, "tp"),
        P("tp"),
        P("tp", None),
        P("tp", None),
    )
    return jax.shard_map(
        on_device, mesh=mesh, in_specs=placed, out_specs=P(("sp", "tp"), None), check_vma=False
    )
```

time: 322 us -> 109 us (0.34)
  waiting for transfers between devices: 122 us -> 0 us
  Pallas kernels: 0 us -> 104 us
  local copies, waits for them, and re-layouts: 65.3 us -> 4.04 us
  matrix products: 52.6 us -> 0 us
  other arithmetic: 46 us -> 0 us
  between operations: 13.6 us -> 0.01 us
  starting transfers between devices: 10.2 us -> 0 us
  blocking collectives: 8.68 us -> 0 us
    pallas_call x0 -> x1, Pallas kernels: none -> 104 us  [on_device(): pl.pallas_call(kernel, out_shape=jax.ShapeDtypeStruct((256, 2048), bf16),...]
    all_gather x3 -> x0, waiting for transfers between devices: 75.4 us -> none  [the longest x2 60.8 us: work_in_pieces(): finished.append(jax.vmap(apply)(lax.all_gather(share, axis), starts))]
    dot_general x63 -> x0, matrix products: 52.6 us -> none  [the longest x12 20.2 us: project(): jnp.dot(normed, weight, preferred_element_type=jnp.float32)]
    reduce_scatter x1 -> x0, waiting for transfers between devices: 46.2 us -> none  [on_device(): lax.psum_scatter((jnp.dot(rec_out, out_rec, preferred_element_type=jnp.fl...]
    dynamic_slice x64 -> x0, local copies, waits for them, and re-layouts: 44.5 us -> none  [local_scan(): lax.scan(advance, (start_state, start_offset), (to_blocks(query), to_bloc...]
    reduce_sum x5 -> x0, other arithmetic: 13 us -> none  [the longest x1 9.47 us: convolve(): jnp.sum(filtered, axis=1)]
    dynamic_update_slice x16 -> x0, other arithmetic: 10.6 us -> none  [local_scan(): lax.scan(advance, (start_state, start_offset), (to_blocks(query), to_bloc...]
    convert_element_type x6 -> x0, other arithmetic: 8.81 us -> none  [the longest x1 3.65 us: convolve(): mixed_in = (glu_value.astype(jnp.float32) * jax.nn.sigmoid(glu_gate.astyp...]
  transfers between devices with their start and end apart: 6 -> 0, of which waited for: 4 -> 0; matrix products, arithmetic and copies ran while one was open for 5% -> 0% of each run, Pallas kernels for 0% -> 0%
where the time goes in v1:
time: 109 us; the launch traced here: 108 us
  Pallas kernels  104 us (95%)
  local copies, waits for them, and re-layouts  4.04 us (4%)
    pallas_call x1, Pallas kernels, on_device(): pl.pallas_call(kernel, out_shape=jax.ShapeDtypeStruct((256, 2048), bf16),...  104 us
    unnamed x2, local copies, waits for them, and re-layouts  4.04 us

profile of v1, /device:TPU:0, one launch (start us, length us, event | category | flops | bytes accessed | tf_op | source)
XLA Modules:
  0.0 108.3 jit_solution(17682755509170448186)
XLA Ops:
  0.0 1.7 %copy.16.shift = f32[1024,4]{1,0:T(8,128)} copy(f32[1024,4]{0,1:T(4,128)} %param.24) | data formatting | bytes 32768 | tf_op args[9]
  1.7 104.3 %shard_map.145 = bf16[256,2048]{1,0:T(8,128)(2,1)} custom-call(bf16[256,2048]{1,0:T(8,128)(2,1)} %tokens.1, f32[1,2048]{1,0:T(1,128)} %bitcast.4, bf16[2048,512]{1,0:T(8,128)(2,1)} %w_query.1, bf16[2048,512]{1,0:T(8,128)(2,1)} %w_forget.1, bf16[2048,512]{1,0:T(8,128)(2,1)} %w_value.1, bf16[2048,512]{1,0:T(8,128)(2,1)} %w_rgate.1, ...), custom_call_target="tpu_custom_call" | custom-call | tf_op jit(solution)/shard_map/pallas_call | solution.py:583
  106.0 2.3 %copy.18 = bf16[256,2048]{1,0:T(8,128)(2,1)} copy(bf16[256,2048]{1,0:T(8,128)(2,1)} %shard_map.145) | data formatting | bytes 2097152

commit v2 on v1

v2 whole, which is shorter than its diff:
```python
import jax
import jax.numpy as jnp
from jax import lax
from jax.experimental import pallas as pl
from jax.experimental.pallas import tpu as pltpu
from jax.sharding import PartitionSpec as P

MESH = pl.DeviceIdType.MESH
HEAD = 128
UNIT = 128
f32 = jnp.float32
bf16 = jnp.bfloat16
scope = jax.named_scope

norm_epsilon = 1e-05
head_epsilon = 1e-06

NT = (((1,), (1,)), ((), ()))
TN = (((0,), (0,)), ((), ()))


def dot(a, b):
    return jnp.dot(a, b, preferred_element_type=f32)


def split3(value):
    hi = value.astype(bf16)
    rest = value - hi.astype(f32)
    mid = rest.astype(bf16)
    low = (rest - mid.astype(f32)).astype(bf16)
    return hi, mid, low


def pack_state(state, log):
    hi, mid, low = split3(log)
    row = lax.broadcasted_iota(jnp.int32, (16, state.shape[1]), 0)
    extra = jnp.where(
        row == 0,
        hi.astype(f32),
        jnp.where(row == 1, mid.astype(f32), jnp.where(row == 2, low.astype(f32), 0.0)),
    )
    return state.astype(bf16), extra.astype(bf16)


def unpack_state(ref):
    state = ref[0:128, :].astype(f32)
    log = jnp.sum(ref[128:144, :].astype(f32), axis=0, keepdims=True)
    return state, log


def kernel(
    tokens,
    norm_gain_hbm,
    w_query,
    w_forget,
    w_value,
    w_rgate,
    w_glu_value,
    w_glu_gate,
    gap_hbm,
    shift_hbm,
    head_gain_hbm,
    taps_hbm,
    conv_gain_hbm,
    out_rec,
    out_conv,
    out,
    norm_gain,
    gap,
    shift,
    head_gain,
    taps,
    conv_gain,
    tok,
    xn,
    xp,
    w_in,
    w_rel,
    raw,
    hml,
    run,
    keys,
    kdec,
    near,
    qfar,
    rgate,
    pad,
    filt,
    s_unit,
    a_unit,
    h_unit,
    s_loc,
    a_loc,
    p_send,
    p_recv,
    y_msg,
    z_msg,
    h_in,
    stat,
    act,
    act_in,
    relay,
    acc,
    load_sem,
    ag_send,
    ag_recv,
    sp_send,
    sp_recv,
    st_send,
    st_recv,
    wx_send,
    wx_recv,
    wp_send,
    wp_recv,
    wc_send,
    wc_recv,
    aa_send,
    aa_recv,
):
    x = lax.axis_index("tp")
    s = lax.axis_index("sp")
    core = lax.rem(s, 2)
    chip = s // 2
    y = lax.rem(chip, 4)
    z = chip // 4

    def around(index, step):
        return lax.rem(index + step, 4)

    right, far, left = around(x, 1), around(x, 2), around(x, 3)
    behind = lax.rem(s + 31, 32)
    ahead = lax.rem(s + 1, 32)
    partner = chip * 2 + (1 - core)

    def at_y(k):
        return (z * 4 + around(y, k)) * 2 + core

    def at_z(k):
        return (around(z, k) * 4 + y) * 2 + core

    barrier = pltpu.get_barrier_semaphore()
    peers = [{"tp": right}, {"tp": left}, {"tp": far}, {"sp": partner}, {"sp": behind}]
    peers += [{"sp": at_y(k)} for k in (1, 2, 3)] + [{"sp": at_z(k)} for k in (1, 2, 3)]
    for peer in peers:
        pl.semaphore_signal(barrier, inc=1, device_id=peer, device_id_type=MESH)

    def remote(src, dst, send_sem, recv_sem, target):
        return pltpu.make_async_remote_copy(
            src_ref=src,
            dst_ref=dst,
            send_sem=send_sem,
            recv_sem=recv_sem,
            device_id=target,
            device_id_type=MESH,
        )

    pairs = [(tokens, tok), (norm_gain_hbm, norm_gain)]
    pairs += [
        (weight, w_in.at[k])
        for k, weight in enumerate(
            (w_forget, w_value, w_query, w_rgate, w_glu_value, w_glu_gate)
        )
    ]
    pairs += [
        (gap_hbm, gap),
        (shift_hbm, shift),
        (head_gain_hbm, head_gain),
        (taps_hbm, taps),
        (conv_gain_hbm, conv_gain),
        (out_rec, w_rel.at[0, 0]),
        (out_conv, w_rel.at[0, 1]),
    ]
    loads = [
        pltpu.make_async_copy(src, dst, load_sem.at[k]) for k, (src, dst) in enumerate(pairs)
    ]
    for load in loads:
        load.start()

    first_index, second_index = (y, z), (z, y)
    first_at, second_at = (at_y, at_z), (at_z, at_y)

    def slice_rows(p, j1, j2):
        return pl.ds(pl.multiple_of(16 * (core * 16 + 4 * j2 + j1), 16), 16)

    own_rows = [slice_rows(p, first_index[p], second_index[p]) for p in (0, 1)]
    weight_of = (out_rec, out_conv)

    def cross(k, p, slot, src, target):
        dst = w_rel.at[slot, p, own_rows[p]]
        return remote(src, dst, wx_send.at[k], wx_recv.at[k], {"tp": target})

    def own_slice(p):
        return weight_of[p].at[own_rows[p]]

    cross_out = [
        cross(0, 0, 3, own_slice(0), right),
        cross(1, 1, 3, own_slice(1), right),
        cross(2, 0, 1, own_slice(0), left),
        cross(3, 1, 1, own_slice(1), left),
        cross(4, 0, 2, w_rel.at[3, 0, own_rows[0]], right),
        cross(5, 1, 2, w_rel.at[1, 1, own_rows[1]], left),
    ]
    cross_in = cross_out

    def packet(p, j1, j2, half):
        cols = pl.ds(0, 2048) if half is None else pl.ds(1024 * half, 1024)
        return w_rel.at[pl.ds(1, 3), p, slice_rows(p, j1, j2), cols]

    def plane(p, k, j1, j2, half, target):
        ref = packet(p, j1, j2, half)
        return remote(ref, ref, wp_send.at[p, k], wp_recv.at[p, k], {"sp": target})

    plane_out, plane_in = [], []
    for p in (0, 1):
        i1, i2 = first_index[p], second_index[p]
        to1, to2 = first_at[p], second_at[p]
        sends = [
            (i1, i2, None, to1(1)),
            (i1, i2, None, to1(3)),
            (around(i1, 3), i2, 0, to1(1)),
            (around(i1, 1), i2, 1, to1(3)),
        ]
        comes = [
            (around(i1, 3), i2, None),
            (around(i1, 1), i2, None),
            (around(i1, 2), i2, 0),
            (around(i1, 2), i2, 1),
        ]
        for m in range(4):
            j1 = around(i1, m)
            sends += [
                (j1, i2, None, to2(1)),
                (j1, i2, None, to2(3)),
                (j1, around(i2, 3), 0, to2(1)),
                (j1, around(i2, 1), 1, to2(3)),
            ]
            comes += [
                (j1, around(i2, 3), None),
                (j1, around(i2, 1), None),
                (j1, around(i2, 2), 0),
                (j1, around(i2, 2), 1),
            ]
        plane_out.append([plane(p, k, *send) for k, send in enumerate(sends)])
        plane_in.append(
            [plane(p, k, *come, sends[k][3]) for k, come in enumerate(comes)]
        )

    def twin(p, n, owner):
        j2 = around(second_index[p], (0, 3, 1, 2)[n])
        rows = pl.ds(pl.multiple_of(256 * owner + 64 * j2, 64), 64)
        ref = w_rel.at[pl.ds(1, 3), p, rows]
        return remote(ref, ref, wc_send.at[p, n], wc_recv.at[p, n], {"sp": partner})

    twin_out = [[twin(p, n, core) for n in range(4)] for p in (0, 1)]
    twin_in = [[twin(p, n, 1 - core) for n in range(4)] for p in (0, 1)]

    def receive(k):
        for p in (1, 0):
            plane_in[p][k].wait_recv()

    def start(*ks):
        for k in ks:
            for p in (1, 0):
                plane_out[p][k].start()

    def weights_0():
        for k in (1, 2, 4, 5):
            cross_in[k].wait_recv()
        start(0, 1, 4, 5)

    def weights_1():
        receive(0)
        receive(1)
        start(2, 3)
        start(16, 17, 8, 9)

    def weights_2():
        receive(2)
        receive(3)
        start(12, 13)
        for p in (1, 0):
            twin_out[p][0].start()

    def weights_3(m):
        receive(4 + 4 * m)
        receive(5 + 4 * m)
        start(6 + 4 * m, 7 + 4 * m)

    def weights_4():
        for p in (1, 0):
            twin_out[p][1].start()
            twin_out[p][2].start()

    def weights_5():
        for m in (0, 3, 1, 2):
            receive(6 + 4 * m)
            receive(7 + 4 * m)
        for p in (1, 0):
            twin_out[p][3].start()

    def norm_rows(piece):
        for row in range(0, UNIT, 32):
            wide = tok[piece * UNIT + row : piece * UNIT + row + 32, :].astype(f32)
            mean = jnp.mean(wide, axis=1, keepdims=True)
            centred = wide - mean
            var = jnp.mean(centred * centred, axis=1, keepdims=True)
            value = centred * lax.rsqrt(var + norm_epsilon) * norm_gain[...]
            xn[2 * x + piece, row : row + 32, :] = value.astype(bf16)

    def send_unit(unit, k, target):
        return remote(
            xn.at[unit], xn.at[unit], ag_send.at[k], ag_recv.at[k], {"tp": target}
        )

    gather = [
        send_unit(2 * x, 0, right),
        send_unit(2 * x + 1, 1, right),
        send_unit(2 * left, 2, right),
        send_unit(2 * x + 1, 3, left),
        send_unit(2 * x, 4, left),
        send_unit(2 * right + 1, 5, left),
    ]
    arrive = [
        send_unit(2 * left, 0, right),
        send_unit(2 * left + 1, 1, right),
        send_unit(2 * far, 2, right),
        send_unit(2 * right + 1, 3, left),
        send_unit(2 * right, 4, left),
        send_unit(2 * far + 1, 5, left),
    ]
    with scope("w_barrier"):
        pl.semaphore_wait(barrier, len(peers))
    for k in range(4):
        cross_out[k].start()
    with scope("w_tok"):
        loads[0].wait()
        loads[1].wait()
    with scope("ln"):
        norm_rows(0)
        norm_rows(1)
    with scope("w_cross"):
        cross_in[0].wait_recv()
        cross_out[4].start()
        cross_in[3].wait_recv()
        cross_out[5].start()
    for k in (0, 3, 1, 4):
        gather[k].start()

    keep = lax.broadcasted_iota(jnp.int32, (UNIT, UNIT), 0) >= lax.broadcasted_iota(
        jnp.int32, (UNIT, UNIT), 1
    )
    ones_low = jnp.where(keep, 1.0, 0.0).astype(bf16)
    tri = jnp.concatenate([ones_low, ones_low, ones_low], axis=1)

    def lanes(h):
        return slice(h * HEAD, (h + 1) * HEAD)

    def units_of(step):
        unit_a = jnp.where(step == 0, 2 * x, jnp.where(step == 1, 2 * left, 2 * left + 1))
        unit_b = jnp.where(step == 0, 2 * x + 1, jnp.where(step == 1, 2 * right + 1, 2 * right))
        return unit_a, unit_b

    def project(*ks):
        for k in ks:
            raw[k] = dot(xp[...], w_in[k]).astype(bf16)

    def each_unit(unit_a, unit_b, body):
        @pl.loop(0, 2)
        def _(k):
            unit = jnp.where(k == 0, unit_a, unit_b)
            body(k, unit, pl.ds(pl.multiple_of(k * UNIT, UNIT), UNIT))

    def gates(k, unit, rows):
        for h in range(4):
            forget = raw[0, rows, lanes(h)].astype(f32)
            gate = gap[:, lanes(h)] * jax.nn.sigmoid(-forget)
            hi, mid, low = split3(jnp.log1p(-gate))
            hml[0:UNIT, lanes(h)] = hi
            hml[UNIT : 2 * UNIT, lanes(h)] = mid
            hml[2 * UNIT : 3 * UNIT, lanes(h)] = low
            keys[:, lanes(h)] = gate
        shifts = shift[:, pl.ds(pl.multiple_of(unit * UNIT, UNIT), UNIT)]
        shifts = jnp.concatenate(split3(shifts), axis=1)
        shift_run = lax.dot_general(tri, shifts, NT, preferred_element_type=f32)
        total = dot(tri, hml[...])
        for h in range(4):
            run_h = total[:, lanes(h)] + shift_run[:, h : h + 1]
            run[k, :, lanes(h)] = run_h
            centre = run_h[63:64, :]
            end = run_h[127:128, :]
            a_unit[unit, :, lanes(h)] = jnp.broadcast_to(end, (8, HEAD))
            decayed = keys[:, lanes(h)] * jnp.exp(centre - run_h)
            kdec[k, :, lanes(h)] = decayed.astype(bf16)
            ending = (decayed * jnp.exp(end - centre)).astype(bf16)
            s_unit[unit, :, lanes(h)] = lax.dot_general(
                raw[1, rows, lanes(h)], ending, TN, preferred_element_type=f32
            )

    def mix(k, unit, rows):
        for h in range(4):
            value = raw[4, rows, lanes(h)].astype(f32)
            mixed = value * jax.nn.sigmoid(raw[5, rows, lanes(h)].astype(f32))
            pad[h, pl.ds(pl.multiple_of(32 + unit * UNIT, 32), UNIT), :] = mixed.astype(
                bf16
            ).astype(f32)

    def scan(k, unit, rows):
        for h in range(4):
            run_h = run[k, :, lanes(h)]
            centre = run_h[63:64, :]
            query = raw[2, rows, lanes(h)].astype(f32)
            query = query * jax.nn.sigmoid(query) * jnp.exp(run_h - centre)
            qfar[unit, :, lanes(h)] = (query * jnp.exp(centre)).astype(bf16)
            scores = lax.dot_general(
                query.astype(bf16), kdec[k, :, lanes(h)], NT, preferred_element_type=f32
            )
            scores = jnp.where(keep, scores, 0.0).astype(bf16)
            near[unit, :, lanes(h)] = dot(scores, raw[1, rows, lanes(h)])
            rgate[unit, :, lanes(h)] = raw[3, rows, lanes(h)]

    @pl.loop(0, 3)
    def _(step):
        unit_a, unit_b = units_of(step)

        @pl.when(step == 0)
        def _():
            with scope("w_weights"):
                for k in range(2, 13):
                    loads[k].wait()

        @pl.when(step == 1)
        def _():
            with scope("w_w0"):
                weights_0()
            with scope("w_ag1"):
                arrive[0].wait_recv()
                gather[2].start()
                arrive[3].wait_recv()
                gather[5].start()

        @pl.when(step == 2)
        def _():
            with scope("w_w2"):
                weights_2()
            with scope("w_ag2"):
                arrive[1].wait_recv()
                arrive[4].wait_recv()

        with scope("proj_fv"):
            xp[0:UNIT, :] = xn[unit_a]
            xp[UNIT : 2 * UNIT, :] = xn[unit_b]
            project(0, 1)
        with scope("gates"):
            each_unit(unit_a, unit_b, gates)

        @pl.when(step == 1)
        def _():
            with scope("w_w1"):
                weights_1()

        @pl.when(step == 2)
        def _():
            with scope("w_w3_0"):
                weights_3(0)

        with scope("proj_rest"):
            project(2, 3, 4, 5)
        with scope("scan"):
            each_unit(unit_a, unit_b, mix)
            each_unit(unit_a, unit_b, scan)

    def sp_copy(src, dst, k, target):
        return remote(src, dst, sp_send.at[k], sp_recv.at[k], {"sp": target})

    pair = sp_copy(p_send, p_recv, 0, partner)
    edge = sp_copy(pad.at[:, pl.ds(1024, 32), :], pad.at[:, pl.ds(0, 32), :], 1, ahead)
    along_y = [sp_copy(y_msg.at[y], y_msg.at[y], 1 + k, at_y(k)) for k in (1, 2, 3)]
    along_z = [sp_copy(z_msg.at[z], z_msg.at[z], 4 + k, at_z(k)) for k in (1, 2, 3)]
    swap = sp_copy(h_in.at[1 - core, core], h_in.at[1 - core, core], 8, partner)

    with scope("w_w3_31"):
        weights_3(3)
        weights_3(1)
    with scope("w_ag3"):
        arrive[2].wait_recv()
        arrive[5].wait_recv()
    unit_a, unit_b = 2 * far, 2 * far + 1
    with scope("proj_fv"):
        xp[0:UNIT, :] = xn[unit_a]
        xp[UNIT : 2 * UNIT, :] = xn[unit_b]
        project(0, 1)
    with scope("gates"):
        each_unit(unit_a, unit_b, gates)
    with scope("combine"):
        state = s_unit[0]
        log = a_unit[0, 0:1, :]
        for u in range(1, 8):
            a_u = a_unit[u, 0:1, :]
            state = state * jnp.exp(a_u) + s_unit[u]
            log = log + a_u
        for half in range(2):
            part_of = slice(half * 256, half * 256 + 256)
            s_loc[half] = state[:, part_of]
            a_loc[half] = jnp.broadcast_to(log[:, part_of], (8, 256))
        body, extra = pack_state(s_loc[1 - core], a_loc[1 - core, 0:1, :])
        p_send[0:128, :] = body
        p_send[128:144, :] = extra
        pair.start()
    with scope("proj_glu"):
        project(4, 5)
        each_unit(unit_a, unit_b, mix)
        edge.start()

    with scope("w_pair"):
        pair.wait()
    mine, mine_log = s_loc[core], a_loc[core, 0:1, :]
    other, other_log = unpack_state(p_recv)
    first = jnp.where(core == 0, mine, other)
    first_log = jnp.where(core == 0, mine_log, other_log)
    second = jnp.where(core == 0, other, mine)
    second_log = jnp.where(core == 0, other_log, mine_log)
    s_loc[core] = first
    a_loc[core] = jnp.broadcast_to(first_log, (8, 256))
    body, extra = pack_state(first * jnp.exp(second_log) + second, first_log + second_log)
    y_msg[y, 0:128, :] = body
    y_msg[y, 128:144, :] = extra
    for copy in along_y:
        copy.start()

    with scope("proj_qr"):
        project(2, 3)
        each_unit(unit_a, unit_b, scan)

    def filter_unit(unit):
        begin = unit * UNIT + 2
        lane = lax.broadcasted_iota(jnp.int32, (UNIT, HEAD), 1)
        sums = jnp.zeros((UNIT, 1), f32)
        squares = jnp.zeros((UNIT, 1), f32)
        for g in range(4):
            total = jnp.zeros((UNIT, HEAD), f32)
            for j in range(31):
                total = total + taps[j : j + 1, lanes(g)] * pad[g, pl.ds(begin + j, UNIT), :]
            filt[unit, :, lanes(g)] = total
            sums = sums + jnp.sum(total, axis=1, keepdims=True)
            squares = squares + jnp.sum(total * total, axis=1, keepdims=True)
        old = stat[0]
        stat[0] = jnp.where(lane == unit, sums, jnp.where(lane == unit + 8, squares, old))

    stat[0] = jnp.zeros((UNIT, HEAD), f32)
    with scope("w_w3_2"):
        weights_3(2)
        weights_4()
    with scope("conv1"):

        @pl.loop(1, 5)
        def _(unit):
            filter_unit(unit)

    with scope("w_y"):
        for copy in along_y:
            copy.wait()
    whole = jnp.zeros((128, 256), f32)
    whole_log = jnp.zeros((1, 256), f32)
    before = jnp.zeros((128, 256), f32)
    before_log = jnp.zeros((1, 256), f32)
    for k in range(4):
        state, log = unpack_state(y_msg.at[k])
        before = jnp.where(k == y, whole, before)
        before_log = jnp.where(k == y, whole_log, before_log)
        whole = whole * jnp.exp(log) + state
        whole_log = whole_log + log
    body, extra = pack_state(whole, whole_log)
    z_msg[z, 0:128, :] = body
    z_msg[z, 128:144, :] = extra
    for copy in along_z:
        copy.start()
    s_loc[1 - core] = before
    a_loc[1 - core] = jnp.broadcast_to(before_log, (8, 256))

    with scope("conv2"):

        @pl.loop(5, 8)
        def _(unit):
            filter_unit(unit)

    with scope("w_edge"):
        edge.wait()

    @pl.when(s == 0)
    def _():
        pad[:, 0:32, :] = jnp.zeros((4, 32, HEAD), f32)

    with scope("conv0"):
        filter_unit(0)

    stats = [
        remote(stat.at[0], stat.at[k], st_send.at[k], st_recv.at[k], {"tp": around(x, k)})
        for k in (1, 2, 3)
    ]
    for copy in stats:
        copy.start()
    with scope("w_w5"):
        weights_5()
    with scope("w_stats"):
        for copy in stats:
            copy.wait()
    stat[0] = (stat[0] + stat[1]) + (stat[2] + stat[3])

    def exchange(p):
        def hop(k, src, dst, target):
            return remote(src, dst, aa_send.at[p, k], aa_recv.at[p, k], {"tp": target})

        low, high = pl.ds(0, UNIT), pl.ds(UNIT, UNIT)
        return [
            hop(0, act.at[2, p, low], relay.at[p, 0], right),
            hop(1, act.at[2, p, high], relay.at[p, 1], left),
            hop(2, act.at[1, p], act_in.at[3, p], right),
            hop(3, act.at[3, p], act_in.at[1, p], left),
            hop(4, relay.at[p, 0], act_in.at[2, p, low], right),
            hop(5, relay.at[p, 1], act_in.at[2, p, high], left),
        ]

    swaps = [exchange(0), exchange(1)]

    def each_row_block(o, body):
        @pl.loop(0, 2)
        def _(k):
            body(o, 2 * around(x, o) + k, pl.ds(pl.multiple_of(k * UNIT, UNIT), UNIT))

    def finish_conv(o, unit, rows):
        lane = lax.broadcasted_iota(jnp.int32, (UNIT, HEAD), 1)
        totals = stat[0]
        sums = jnp.sum(jnp.where(lane == unit, totals, 0.0), axis=1, keepdims=True)
        squares = jnp.sum(jnp.where(lane == unit + 8, totals, 0.0), axis=1, keepdims=True)
        mean = sums * (1.0 / 2048)
        scale = lax.rsqrt(squares * (1.0 / 2048) - mean * mean + norm_epsilon)
        for h in range(4):
            conv = (filt[unit, :, lanes(h)] - mean) * scale * conv_gain[:, lanes(h)]
            act[o, 1, rows, lanes(h)] = (conv * jax.nn.sigmoid(conv)).astype(bf16)

    def finish_rec(o, unit, rows):
        for h in range(4):
            rec = near[unit, :, lanes(h)] + lax.dot_general(
                qfar[unit, :, lanes(h)],
                h_unit[unit, :, lanes(h)],
                NT,
                preferred_element_type=f32,
            )
            power = jnp.mean(rec * rec, axis=1, keepdims=True)
            gate = rgate[unit, :, lanes(h)].astype(f32)
            rec = rec * lax.rsqrt(power + head_epsilon) * head_gain[...]
            act[o, 0, rows, lanes(h)] = (rec * (gate * jax.nn.sigmoid(gate))).astype(bf16)

    def finish_and_send(p, body):
        each_row_block(2, body)
        swaps[p][0].start()
        swaps[p][1].start()
        each_row_block(1, body)
        swaps[p][2].start()
        each_row_block(3, body)
        swaps[p][3].start()
        each_row_block(0, body)

    with scope("fin_conv"):
        finish_and_send(1, finish_conv)

    with scope("w_z"):
        for copy in along_z:
            copy.wait()
    whole = jnp.zeros((128, 256), f32)
    before = jnp.zeros((128, 256), f32)
    for k in range(4):
        state, log = unpack_state(z_msg.at[k])
        before = jnp.where(k == z, whole, before)
        whole = whole * jnp.exp(log) + state
    chip_in = before * jnp.exp(a_loc[1 - core, 0:1, :]) + s_loc[1 - core]
    h_in[0, core] = chip_in
    h_in[1, core] = chip_in * jnp.exp(a_loc[core, 0:1, :]) + s_loc[core]
    swap.start()
    with scope("w_relay_conv"):
        swaps[1][0].wait_recv()
        swaps[1][4].start()
        swaps[1][1].wait_recv()
        swaps[1][5].start()
    with scope("w_swap"):
        swap.wait()

    with scope("h_units"):
        state = jnp.concatenate([h_in[core, 0], h_in[core, 1]], axis=1)
        for u in range(8):
            h_unit[u] = state.astype(bf16)
            if u < 7:
                state = state * jnp.exp(a_unit[u, 0:1, :]) + s_unit[u]

    with scope("fin_rec"):
        finish_and_send(0, finish_rec)

    def add_product(k, p, begin):
        source = act.at[0, p] if k == 0 else act_in.at[k, p]
        for c in range(4):
            cols = slice(c * 512, c * 512 + 512)
            product = dot(source[...], w_rel[k, p, :, cols])
            acc[:, cols] = product if begin else acc[:, cols] + product

    with scope("w_twin"):
        loads[13].wait()
        loads[14].wait()
        for p in (1, 0):
            for n in range(4):
                twin_in[p][n].wait_recv()
    with scope("dot_conv"):
        add_product(0, 1, True)
        swaps[1][2].wait_recv()
        add_product(3, 1, False)
        swaps[1][3].wait_recv()
        add_product(1, 1, False)
    with scope("w_relay_rec"):
        swaps[0][0].wait_recv()
        swaps[0][4].start()
        swaps[0][1].wait_recv()
        swaps[0][5].start()
    with scope("dot_conv2"):
        swaps[1][4].wait_recv()
        swaps[1][5].wait_recv()
        add_product(2, 1, False)
        add_product(0, 0, False)
    with scope("dot_rec"):
        swaps[0][2].wait_recv()
        add_product(3, 0, False)
        swaps[0][3].wait_recv()
        add_product(1, 0, False)
    with scope("w_rec2"):
        swaps[0][4].wait_recv()
        swaps[0][5].wait_recv()
    with scope("dot_last"):
        for c in range(4):
            cols = slice(c * 512, c * 512 + 512)
            product = dot(act_in[2, 0], w_rel[2, 0, :, cols])
            out[:, cols] = (acc[:, cols] + product).astype(bf16)

    with scope("w_sends"):
        for copy in gather + cross_out + plane_out[0] + plane_out[1]:
            copy.wait_send()
        for copy in twin_out[0] + twin_out[1] + swaps[0] + swaps[1]:
            copy.wait_send()


def on_device(
    tokens,
    norm_gain,
    w_query,
    w_forget,
    w_value,
    w_rgate,
    w_glu_value,
    w_glu_gate,
    forget_gap,
    decay_shift,
    head_gain,
    conv_taps,
    conv_gain,
    out_rec,
    out_conv,
):
    vmem = pl.BlockSpec(memory_space=pltpu.VMEM)
    hbm = pl.BlockSpec(memory_space=pl.ANY)
    dma = pltpu.SemaphoreType.DMA
    scratch = [
        pltpu.VMEM((1, 2048), f32),
        pltpu.VMEM((1, 512), f32),
        pltpu.VMEM((4, 1024), f32),
        pltpu.VMEM((1, 128), f32),
        pltpu.VMEM((31, 512), f32),
        pltpu.VMEM((1, 512), f32),
        pltpu.VMEM((256, 2048), bf16),
        pltpu.VMEM((8, 128, 2048), bf16),
        pltpu.VMEM((256, 2048), bf16),
        pltpu.VMEM((6, 2048, 512), bf16),
        pltpu.VMEM((4, 2, 512, 2048), bf16),
        pltpu.VMEM((6, 256, 512), bf16),
        pltpu.VMEM((384, 512), bf16),
        pltpu.VMEM((2, 128, 512), f32),
        pltpu.VMEM((128, 512), f32),
        pltpu.VMEM((2, 128, 512), bf16),
        pltpu.VMEM((8, 128, 512), f32),
        pltpu.VMEM((8, 128, 512), bf16),
        pltpu.VMEM((8, 128, 512), bf16),
        pltpu.VMEM((4, 1056, 128), f32),
        pltpu.VMEM((8, 128, 512), f32),
        pltpu.VMEM((8, 128, 512), f32),
        pltpu.VMEM((8, 8, 512), f32),
        pltpu.VMEM((8, 128, 512), bf16),
        pltpu.VMEM((2, 128, 256), f32),
        pltpu.VMEM((2, 8, 256), f32),
        pltpu.VMEM((144, 256), bf16),
        pltpu.VMEM((144, 256), bf16),
        pltpu.VMEM((4, 144, 256), bf16),
        pltpu.VMEM((4, 144, 256), bf16),
        pltpu.VMEM((2, 2, 128, 256), f32),
        pltpu.VMEM((4, 128, 128), f32),
        pltpu.VMEM((4, 2, 256, 512), bf16),
        pltpu.VMEM((4, 2, 256, 512), bf16),
        pltpu.VMEM((2, 2, 128, 512), bf16),
        pltpu.VMEM((256, 2048), f32),
        dma((15,)),
        dma((6,)),
        dma((6,)),
        dma((9,)),
        dma((9,)),
        dma((4,)),
        dma((4,)),
        dma((6,)),
        dma((6,)),
        dma((2, 20)),
        dma((2, 20)),
        dma((2, 4)),
        dma((2, 4)),
        dma((2, 6)),
        dma((2, 6)),
    ]
    return pl.pallas_call(
        kernel,
        out_shape=jax.ShapeDtypeStruct((256, 2048), bf16),
        in_specs=[hbm] * 15,
        out_specs=vmem,
        scratch_shapes=scratch,
        compiler_params=pltpu.CompilerParams(
            collective_id=0, has_side_effects=True, vmem_limit_bytes=62 * 1024 * 1024
        ),
    )(
        tokens,
        norm_gain[None],
        w_query,
        w_forget,
        w_value,
        w_rgate,
        w_glu_value,
        w_glu_gate,
        forget_gap[None],
        decay_shift.T,
        head_gain[None],
        conv_taps,
        conv_gain[None],
        out_rec,
        out_conv,
    )


def solution(mesh):
    placed = (
        P(("sp", "tp"), None),
        P(),
        P(None, "tp"),
        P(None, "tp"),
        P(None, "tp"),
        P(None, "tp"),
        P(None, "tp"),
        P(None, "tp"),
        P("tp"),
        P("sp", "tp"),
        P(),
        P(None, "tp"),
        P("tp"),
        P("tp", None),
        P("tp", None),
    )
    return jax.shard_map(
        on_device, mesh=mesh, in_specs=placed, out_specs=P(("sp", "tp"), None), check_vma=False
    )
```

time: 109 us -> 94 us (0.86)
  Pallas kernels: 104 us -> 91.6 us
  local copies, waits for them, and re-layouts: 4.04 us -> 2.3 us
    pallas_call x1, Pallas kernels: 104 us -> 91.6 us  [on_device(): pl.pallas_call(kernel, out_shape=jax.ShapeDtypeStruct((256, 2048), bf16),...]
    unnamed x2 -> x1, local copies, waits for them, and re-layouts: 4.04 us -> 2.3 us
where the time goes in v2:
time: 94 us; the launch traced here: 93.9 us
  Pallas kernels  91.6 us (97%)
  local copies, waits for them, and re-layouts  2.3 us (2%)
    pallas_call x1, Pallas kernels, on_device(): pl.pallas_call(kernel, out_shape=jax.ShapeDtypeStruct((256, 2048), bf16),...  91.6 us
    unnamed x1, local copies, waits for them, and re-layouts  2.3 us

profile of v2, /device:TPU:0, one launch (start us, length us, event | category | flops | bytes accessed | tf_op | source)
XLA Modules:
  0.0 93.9 jit_solution(13516889812850435396)
XLA Ops:
  0.0 91.6 %shard_map.145 = bf16[256,2048]{1,0:T(8,128)(2,1)} custom-call(bf16[256,2048]{1,0:T(8,128)(2,1)} %tokens.1, f32[1,2048]{1,0:T(1,128)} %bitcast.6, bf16[2048,512]{1,0:T(8,128)(2,1)} %w_query.1, bf16[2048,512]{1,0:T(8,128)(2,1)} %w_forget.1, bf16[2048,512]{1,0:T(8,128)(2,1)} %w_value.1, bf16[2048,512]{1,0:T(8,128)(2,1)} %w_rgate.1, ...), custom_call_target="tpu_custom_call" | custom-call | tf_op jit(solution)/shard_map/pallas_call | solution.py:821
  91.6 2.3 %copy.17 = bf16[256,2048]{1,0:T(8,128)(2,1)} copy(bf16[256,2048]{1,0:T(8,128)(2,1)} %shard_map.145) | data formatting | bytes 2097152

commit v3 on v2

v3 whole, which is shorter than its diff:
```python
import jax
import jax.numpy as jnp
from jax import lax
from jax.experimental import pallas as pl
from jax.experimental.pallas import tpu as pltpu
from jax.sharding import PartitionSpec as P

MESH = pl.DeviceIdType.MESH
HEAD = 128
UNIT = 128
f32 = jnp.float32
bf16 = jnp.bfloat16
scope = jax.named_scope

norm_epsilon = 1e-05
head_epsilon = 1e-06

NT = (((1,), (1,)), ((), ()))
TN = (((0,), (0,)), ((), ()))


def dot(a, b):
    return jnp.dot(a, b, preferred_element_type=f32)


def split3(value):
    hi = value.astype(bf16)
    rest = value - hi.astype(f32)
    mid = rest.astype(bf16)
    low = (rest - mid.astype(f32)).astype(bf16)
    return hi, mid, low


def pack_state(state, log):
    hi, mid, low = split3(log)
    row = lax.broadcasted_iota(jnp.int32, (16, state.shape[1]), 0)
    extra = jnp.where(
        row == 0,
        hi.astype(f32),
        jnp.where(row == 1, mid.astype(f32), jnp.where(row == 2, low.astype(f32), 0.0)),
    )
    return state.astype(bf16), extra.astype(bf16)


def unpack_state(ref):
    state = ref[0:128, :].astype(f32)
    log = jnp.sum(ref[128:144, :].astype(f32), axis=0, keepdims=True)
    return state, log


def kernel(
    tokens,
    norm_gain_hbm,
    w_query,
    w_forget,
    w_value,
    w_rgate,
    w_glu_value,
    w_glu_gate,
    gap_hbm,
    shift_hbm,
    head_gain_hbm,
    taps_hbm,
    conv_gain_hbm,
    out_rec,
    out_conv,
    out,
    norm_gain,
    gap,
    shift,
    head_gain,
    taps,
    conv_gain,
    tok,
    xn,
    xp,
    w_in,
    w_rel,
    raw,
    hml,
    run,
    keys,
    kdec,
    near,
    qfar,
    rgate,
    filt,
    s_unit,
    a_unit,
    h_unit,
    s_loc,
    a_loc,
    p_send,
    p_recv,
    y_msg,
    z_msg,
    h_in,
    act,
    act_in,
    relay,
    acc,
    w_own,
    mixed_in,
    c_in,
    c_pad,
    c_act,
    tg,
    load_sem,
    ag_send,
    ag_recv,
    sp_send,
    sp_recv,
    st_send,
    st_recv,
    wx_send,
    wx_recv,
    wp_send,
    wp_recv,
    wc_send,
    wc_recv,
    aa_send,
    aa_recv,
):
    x = lax.axis_index("tp")
    s = lax.axis_index("sp")
    core = lax.rem(s, 2)
    chip = s // 2
    y = lax.rem(chip, 4)
    z = chip // 4

    def around(index, step):
        return lax.rem(index + step, 4)

    right, far, left = around(x, 1), around(x, 2), around(x, 3)
    behind = lax.rem(s + 31, 32)
    ahead = lax.rem(s + 1, 32)
    partner = chip * 2 + (1 - core)

    def at_y(k):
        return (z * 4 + around(y, k)) * 2 + core

    def at_z(k):
        return (around(z, k) * 4 + y) * 2 + core

    barrier = pltpu.get_barrier_semaphore()
    peers = [{"tp": right}, {"tp": left}, {"tp": far}, {"sp": partner}, {"sp": behind}]
    peers += [{"sp": at_y(k)} for k in (1, 2, 3)] + [{"sp": at_z(k)} for k in (1, 2, 3)]
    for peer in peers:
        pl.semaphore_signal(barrier, inc=1, device_id=peer, device_id_type=MESH)

    def remote(src, dst, send_sem, recv_sem, target):
        return pltpu.make_async_remote_copy(
            src_ref=src,
            dst_ref=dst,
            send_sem=send_sem,
            recv_sem=recv_sem,
            device_id=target,
            device_id_type=MESH,
        )

    first_index, second_index = (y, z), (z, y)
    first_at, second_at = (at_y, at_z), (at_z, at_y)

    def slice_rows(p, j1, j2):
        return pl.ds(pl.multiple_of(16 * (core * 16 + 4 * j2 + j1), 16), 16)

    own_rows = [slice_rows(p, first_index[p], second_index[p]) for p in (0, 1)]
    weight_of = (out_rec, out_conv)

    own_loads = [
        pltpu.make_async_copy(weight_of[p].at[own_rows[p]], w_own.at[p], load_sem.at[15 + p])
        for p in (0, 1)
    ]
    pairs = [(tokens, tok), (norm_gain_hbm, norm_gain)]
    pairs += [
        (weight, w_in.at[k])
        for k, weight in enumerate(
            (w_forget, w_value, w_query, w_rgate, w_glu_value, w_glu_gate)
        )
    ]
    pairs += [
        (gap_hbm, gap),
        (shift_hbm, shift),
        (head_gain_hbm, head_gain),
        (taps_hbm, taps),
        (conv_gain_hbm, conv_gain),
        (out_rec, w_rel.at[0, 0]),
        (out_conv, w_rel.at[0, 1]),
    ]
    loads = [
        pltpu.make_async_copy(src, dst, load_sem.at[k]) for k, (src, dst) in enumerate(pairs)
    ]
    for load in own_loads + loads:
        load.start()

    def cross(k, p, slot, src, target):
        dst = w_rel.at[slot, p, own_rows[p]]
        return remote(src, dst, wx_send.at[k], wx_recv.at[k], {"tp": target})

    def own_slice(p):
        return w_own.at[p]

    cross_out = [
        cross(0, 0, 3, own_slice(0), right),
        cross(1, 1, 3, own_slice(1), right),
        cross(2, 0, 1, own_slice(0), left),
        cross(3, 1, 1, own_slice(1), left),
        cross(4, 0, 2, w_rel.at[3, 0, own_rows[0]], right),
        cross(5, 1, 2, w_rel.at[1, 1, own_rows[1]], left),
    ]
    cross_in = cross_out

    def packet(p, j1, j2, half):
        cols = pl.ds(0, 2048) if half is None else pl.ds(1024 * half, 1024)
        return w_rel.at[pl.ds(1, 3), p, slice_rows(p, j1, j2), cols]

    def plane(p, k, j1, j2, half, target):
        ref = packet(p, j1, j2, half)
        return remote(ref, ref, wp_send.at[p, k], wp_recv.at[p, k], {"sp": target})

    plane_out, plane_in = [], []
    for p in (0, 1):
        i1, i2 = first_index[p], second_index[p]
        to1, to2 = first_at[p], second_at[p]
        sends = [
            (i1, i2, None, to1(1)),
            (i1, i2, None, to1(3)),
            (around(i1, 3), i2, 0, to1(1)),
            (around(i1, 1), i2, 1, to1(3)),
        ]
        comes = [
            (around(i1, 3), i2, None),
            (around(i1, 1), i2, None),
            (around(i1, 2), i2, 0),
            (around(i1, 2), i2, 1),
        ]
        for m in range(4):
            j1 = around(i1, m)
            sends += [
                (j1, i2, None, to2(1)),
                (j1, i2, None, to2(3)),
                (j1, around(i2, 3), 0, to2(1)),
                (j1, around(i2, 1), 1, to2(3)),
            ]
            comes += [
                (j1, around(i2, 3), None),
                (j1, around(i2, 1), None),
                (j1, around(i2, 2), 0),
                (j1, around(i2, 2), 1),
            ]
        plane_out.append([plane(p, k, *send) for k, send in enumerate(sends)])
        plane_in.append(
            [plane(p, k, *come, sends[k][3]) for k, come in enumerate(comes)]
        )

    def twin(p, n, owner):
        j2 = around(second_index[p], (0, 3, 1, 2)[n])
        rows = pl.ds(pl.multiple_of(256 * owner + 64 * j2, 64), 64)
        ref = w_rel.at[pl.ds(1, 3), p, rows]
        return remote(ref, ref, wc_send.at[p, n], wc_recv.at[p, n], {"sp": partner})

    twin_out = [[twin(p, n, core) for n in range(4)] for p in (0, 1)]
    twin_in = [[twin(p, n, 1 - core) for n in range(4)] for p in (0, 1)]

    def receive(k):
        for p in (1, 0):
            plane_in[p][k].wait_recv()

    def start(*ks):
        for k in ks:
            for p in (1, 0):
                plane_out[p][k].start()

    def weights_0():
        for k in (1, 2, 4, 5):
            cross_in[k].wait_recv()
        start(0, 1, 4, 5)

    def weights_1():
        receive(0)
        receive(1)
        start(2, 3)
        start(16, 17, 8, 9)

    def weights_2():
        receive(2)
        receive(3)
        start(12, 13)
        for p in (1, 0):
            twin_out[p][0].start()

    def weights_3(m):
        receive(4 + 4 * m)
        receive(5 + 4 * m)
        start(6 + 4 * m, 7 + 4 * m)

    def weights_4():
        for p in (1, 0):
            twin_out[p][1].start()
            twin_out[p][2].start()

    def weights_5():
        for m in (0, 3, 1, 2):
            receive(6 + 4 * m)
            receive(7 + 4 * m)
        for p in (1, 0):
            twin_out[p][3].start()

    def norm_rows(piece):
        for row in range(0, UNIT, 32):
            wide = tok[piece * UNIT + row : piece * UNIT + row + 32, :].astype(f32)
            mean = jnp.mean(wide, axis=1, keepdims=True)
            centred = wide - mean
            var = jnp.mean(centred * centred, axis=1, keepdims=True)
            value = centred * lax.rsqrt(var + norm_epsilon) * norm_gain[...]
            xn[2 * x + piece, row : row + 32, :] = value.astype(bf16)

    def rows_copy(unit, begin, size, k, way):
        ref = xn.at[unit, pl.ds(begin, size)]
        target = {"tp": left if way else right}
        return remote(ref, ref, ag_send.at[way, k], ag_recv.at[way, k], target)

    parts = (
        ((1, 0, 32), (1, 32, 32), (1, 64, 64), (0, 0, 64), (0, 64, 64), (0, 0, 64), (1, 0, 64)),
        ((0, 64, 32), (0, 96, 32), (0, 0, 64), (1, 64, 64), (1, 0, 64), (0, 64, 64), (1, 64, 64)),
    )
    gather, arrive = [], []
    for way in (0, 1):
        source = left if way == 0 else right
        gather.append(
            [
                rows_copy(2 * (x if k < 5 else source) + u, begin, size, k, way)
                for k, (u, begin, size) in enumerate(parts[way])
            ]
        )
        arrive.append(
            [
                rows_copy(2 * (source if k < 5 else far) + u, begin, size, k, way)
                for k, (u, begin, size) in enumerate(parts[way])
            ]
        )

    def tokens_in(*ks):
        for k in ks:
            arrive[0][k].wait_recv()
            arrive[1][k].wait_recv()

    loads[0].wait()
    loads[1].wait()
    with scope("ln"):
        norm_rows(0)
        norm_rows(1)
    with scope("w_barrier"):
        pl.semaphore_wait(barrier, len(peers))
    for load in own_loads:
        load.wait()
    for k in range(4):
        cross_out[k].start()
    gather[0][0].start()
    gather[1][0].start()
    with scope("w_cross"):
        cross_in[0].wait_recv()
        cross_out[4].start()
        cross_in[3].wait_recv()
        cross_out[5].start()
    for k in range(1, 5):
        gather[0][k].start()
        gather[1][k].start()

    keep = lax.broadcasted_iota(jnp.int32, (UNIT, UNIT), 0) >= lax.broadcasted_iota(
        jnp.int32, (UNIT, UNIT), 1
    )
    ones_low = jnp.where(keep, 1.0, 0.0).astype(bf16)
    tri = jnp.concatenate([ones_low, ones_low, ones_low], axis=1)

    def lanes(h):
        return slice(h * HEAD, (h + 1) * HEAD)

    def units_of(step):
        unit_a = jnp.where(step == 0, 2 * x, jnp.where(step == 1, 2 * left + 1, 2 * left))
        unit_b = jnp.where(step == 0, 2 * x + 1, jnp.where(step == 1, 2 * right, 2 * right + 1))
        return unit_a, unit_b

    def project(*ks):
        for k in ks:
            raw[k] = dot(xp[...], w_in[k]).astype(bf16)

    def each_unit(unit_a, unit_b, body):
        for k, unit in enumerate((unit_a, unit_b)):
            body(k, unit, pl.ds(k * UNIT, UNIT))

    def gates(k, unit, rows):
        for h in range(4):
            forget = raw[0, rows, lanes(h)].astype(f32)
            gate = gap[:, lanes(h)] * jax.nn.sigmoid(-forget)
            hi, mid, low = split3(jnp.log1p(-gate))
            hml[k, 0:UNIT, lanes(h)] = hi
            hml[k, UNIT : 2 * UNIT, lanes(h)] = mid
            hml[k, 2 * UNIT : 3 * UNIT, lanes(h)] = low
            keys[k, :, lanes(h)] = gate
        shifts = shift[:, pl.ds(pl.multiple_of(unit * UNIT, UNIT), UNIT)]
        shifts = jnp.concatenate(split3(shifts), axis=1)
        shift_run = lax.dot_general(tri, shifts, NT, preferred_element_type=f32)
        total = dot(tri, hml[k])
        for h in range(4):
            run_h = total[:, lanes(h)] + shift_run[:, h : h + 1]
            run[k, :, lanes(h)] = run_h
            centre = run_h[63:64, :]
            end = run_h[127:128, :]
            a_unit[unit, :, lanes(h)] = jnp.broadcast_to(end, (8, HEAD))
            decayed = keys[k, :, lanes(h)] * jnp.exp(centre - run_h)
            kdec[k, :, lanes(h)] = decayed.astype(bf16)
            ending = (decayed * jnp.exp(end - centre)).astype(bf16)
            s_unit[unit, :, lanes(h)] = lax.dot_general(
                raw[1, rows, lanes(h)], ending, TN, preferred_element_type=f32
            )

    def mix(k, unit, rows):
        value = raw[4, rows, :].astype(f32)
        mixed = value * jax.nn.sigmoid(raw[5, rows, :].astype(f32))
        mixed_in[pl.ds(pl.multiple_of(32 + unit * UNIT, 32), UNIT), :] = mixed.astype(bf16)

    def scan(k, unit, rows):
        for h in range(4):
            run_h = run[k, :, lanes(h)]
            centre = run_h[63:64, :]
            query = raw[2, rows, lanes(h)].astype(f32)
            query = query * jax.nn.sigmoid(query) * jnp.exp(run_h - centre)
            qfar[unit, :, lanes(h)] = (query * jnp.exp(centre)).astype(bf16)
            scores = lax.dot_general(
                query.astype(bf16), kdec[k, :, lanes(h)], NT, preferred_element_type=f32
            )
            scores = jnp.where(keep, scores, 0.0).astype(bf16)
            near[unit, :, lanes(h)] = dot(scores, raw[1, rows, lanes(h)])
            rgate[unit, :, lanes(h)] = raw[3, rows, lanes(h)]

    def sp_copy(src, dst, k, target):
        return remote(src, dst, sp_send.at[k], sp_recv.at[k], {"sp": target})

    edge = sp_copy(mixed_in.at[pl.ds(1024, 32)], mixed_in.at[pl.ds(0, 32)], 1, ahead)

    def send_edge(owner):
        @pl.when(x == owner)
        def _():
            edge.start()

    def rows_of(o, begin, size):
        return mixed_in.at[pl.ds(pl.multiple_of(256 * around(x, o) + begin, 32), size)]

    def hop(p, k, src, dst, target):
        return remote(src, dst, aa_send.at[p, k], aa_recv.at[p, k], {"tp": target})

    low, high = pl.ds(0, UNIT), pl.ds(UNIT, UNIT)
    low_in, high_in = pl.ds(32, UNIT), pl.ds(32 + UNIT, UNIT)
    gated = [
        hop(1, 0, rows_of(2, 32, UNIT), relay.at[1, 0], left),
        hop(1, 1, rows_of(2, 32 + UNIT, UNIT), relay.at[1, 1], right),
        hop(1, 2, rows_of(1, 32, UNIT), c_in.at[3, low_in], right),
        hop(1, 3, rows_of(1, 32 + UNIT, UNIT), c_in.at[3, high_in], right),
        hop(1, 4, rows_of(3, 32, UNIT), c_in.at[1, low_in], left),
        hop(1, 5, rows_of(3, 32 + UNIT, UNIT), c_in.at[1, high_in], left),
        hop(1, 6, relay.at[1, 0], c_in.at[2, low_in], left),
        hop(1, 7, relay.at[1, 1], c_in.at[2, high_in], right),
    ]
    edges = [
        hop(1, 7 + o, rows_of(o, 0, 32), c_in.at[4 - o, pl.ds(0, 32)], {1: right, 2: far, 3: left}[o])
        for o in (1, 2, 3)
    ]
    acts = [
        hop(0, 0, act.at[2, low], relay.at[0, 0], left),
        hop(0, 1, act.at[2, high], relay.at[0, 1], right),
        hop(0, 2, act.at[1, low], act_in.at[3, low], right),
        hop(0, 3, act.at[1, high], act_in.at[3, high], right),
        hop(0, 4, act.at[3, low], act_in.at[1, low], left),
        hop(0, 5, act.at[3, high], act_in.at[1, high], left),
        hop(0, 6, relay.at[0, 0], act_in.at[2, low], left),
        hop(0, 7, relay.at[0, 1], act_in.at[2, high], right),
    ]
    filters = [
        remote(tg.at[0], tg.at[4 - j], st_send.at[j], st_recv.at[j], {"tp": around(x, j)})
        for j in (1, 2, 3)
    ]

    @pl.loop(0, 3)
    def _(step):
        unit_a, unit_b = units_of(step)

        @pl.when(step == 0)
        def _():
            with scope("w_weights"):
                for k in range(2, 13):
                    loads[k].wait()
            tg[0, 0:31, :] = taps[...]
            tg[0, 31:32, :] = conv_gain[...]

        @pl.when(step == 1)
        def _():
            with scope("w_ag1"):
                tokens_in(0, 1)
                gather[1][5].start()
                tokens_in(2)

        @pl.when(step == 2)
        def _():
            with scope("w_ag2"):
                tokens_in(3)
                gather[0][5].start()
                gather[0][6].start()
                gather[1][6].start()
                for copy in filters:
                    copy.start()
                tokens_in(4)
            with scope("w_w2"):
                weights_2()
                weights_3(0)

        with scope("proj_fv"):
            xp[0:UNIT, :] = xn[unit_a]
            xp[UNIT : 2 * UNIT, :] = xn[unit_b]
            project(0, 1)

        @pl.when(step == 1)
        def _():
            with scope("w_w1"):
                weights_1()

        with scope("gates"):
            each_unit(unit_a, unit_b, gates)

        with scope("proj_rest"):
            project(2, 3, 4, 5)

        @pl.when(step == 0)
        def _():
            with scope("w_w0"):
                weights_0()

        with scope("scan"):
            each_unit(unit_a, unit_b, mix)
            each_unit(unit_a, unit_b, scan)

        @pl.when(step == 0)
        def _():
            send_edge(3)

        @pl.when(step == 1)
        def _():
            send_edge(0)

        @pl.when(step == 2)
        def _():
            send_edge(2)

    unit_rows = pl.ds(0, UNIT)

    def project_unit(unit, *ks):
        for k in ks:
            raw[k, 0:UNIT, :] = dot(xn[unit], w_in[k]).astype(bf16)

    with scope("w_w3_31"):
        weights_3(3)
        weights_3(1)
    with scope("w_far_a"):
        tokens_in(5)
    with scope("far_a"):
        project_unit(2 * far, 0, 1)
        gates(0, 2 * far, unit_rows)
        project_unit(2 * far, 2, 3, 4, 5)
        mix(0, 2 * far, unit_rows)
        scan(0, 2 * far, unit_rows)
    with scope("w_far_b"):
        tokens_in(6)
    with scope("far_b"):
        project_unit(2 * far + 1, 0, 1)
        gates(0, 2 * far + 1, unit_rows)

    pair = sp_copy(p_send, p_recv, 0, partner)
    along_y = [
        [sp_copy(y_msg.at[y, hd], y_msg.at[y, hd], 1 + 3 * hd + k, at_y(k)) for k in (2, 1, 3)]
        for hd in (0, 1)
    ]
    along_z = [
        [sp_copy(z_msg.at[z, hd], z_msg.at[z, hd], 7 + 3 * hd + k, at_z(k)) for k in (2, 1, 3)]
        for hd in (0, 1)
    ]
    swap = sp_copy(h_in.at[1 - core, core], h_in.at[1 - core, core], 14, partner)

    with scope("combine"):
        state = s_unit[0]
        log = a_unit[0, 0:1, :]
        for u in range(1, 8):
            a_u = a_unit[u, 0:1, :]
            state = state * jnp.exp(a_u) + s_unit[u]
            log = log + a_u
        for half in range(2):
            part_of = slice(half * 256, half * 256 + 256)
            s_loc[half] = state[:, part_of]
            a_loc[half] = jnp.broadcast_to(log[:, part_of], (8, 256))
        body, extra = pack_state(s_loc[1 - core], a_loc[1 - core, 0:1, :])
        p_send[0:128, :] = body
        p_send[128:144, :] = extra
        pair.start()
    with scope("w_pair"):
        pair.wait()
    mine, mine_log = s_loc[core], a_loc[core, 0:1, :]
    other, other_log = unpack_state(p_recv)
    first = jnp.where(core == 0, mine, other)
    first_log = jnp.where(core == 0, mine_log, other_log)
    second = jnp.where(core == 0, other, mine)
    second_log = jnp.where(core == 0, other_log, mine_log)
    s_loc[core] = first
    a_loc[core] = jnp.broadcast_to(first_log, (8, 256))
    both = first * jnp.exp(second_log) + second
    both_log = first_log + second_log
    for hd in (0, 1):
        body, extra = pack_state(both[:, lanes(hd)], both_log[:, lanes(hd)])
        y_msg[y, hd, 0:128, :] = body
        y_msg[y, hd, 128:144, :] = extra
        for copy in along_y[hd]:
            copy.start()

    for k in (0, 2, 4, 5):
        gated[k].start()
    with scope("proj_glu"):
        project_unit(2 * far + 1, 4, 5)
        mix(0, 2 * far + 1, unit_rows)
        send_edge(1)
        gated[1].start()
        gated[3].start()

    with scope("w_w3_2"):
        weights_3(2)
        weights_4()

    with scope("proj_qr"):
        project_unit(2 * far + 1, 2, 3)
        scan(0, 2 * far + 1, unit_rows)

    def widen(k, begin, size):
        if k == 0:
            source = rows_of(0, begin, size)[...]
        else:
            source = c_in[k, begin : begin + size, :]
        for g in range(4):
            c_pad[4 * k + g, begin : begin + size, :] = source[:, lanes(g)].astype(f32)

    def filter_rows(k, u):
        for g in range(4):
            total = jnp.zeros((UNIT, HEAD), f32)
            for j in range(31):
                begin = u * UNIT + 2 + j
                total = (
                    total
                    + tg[k, j : j + 1, lanes(g)] * c_pad[4 * k + g, begin : begin + UNIT, :]
                )
            filt[u, :, lanes(4 * k + g)] = total

    with scope("w_edge"):
        edge.wait_recv()

        @pl.when(s == 0)
        def _():
            mixed_in[0:32, :] = jnp.zeros((32, 512), bf16)

    for copy in edges:
        copy.start()
    with scope("conv_0"):
        widen(0, 0, 288)
        filter_rows(0, 0)
        filter_rows(0, 1)

    for hd in (0, 1):
        with scope("w_y"):
            for copy in along_y[hd]:
                copy.wait()
        whole = jnp.zeros((128, HEAD), f32)
        whole_log = jnp.zeros((1, HEAD), f32)
        before = jnp.zeros((128, HEAD), f32)
        before_log = jnp.zeros((1, HEAD), f32)
        for k in range(4):
            state, log = unpack_state(y_msg.at[k, hd])
            before = jnp.where(k == y, whole, before)
            before_log = jnp.where(k == y, whole_log, before_log)
            whole = whole * jnp.exp(log) + state
            whole_log = whole_log + log
        body, extra = pack_state(whole, whole_log)
        z_msg[z, hd, 0:128, :] = body
        z_msg[z, hd, 128:144, :] = extra
        for copy in along_z[hd]:
            copy.start()
        s_loc[1 - core, :, lanes(hd)] = before
        a_loc[1 - core, :, lanes(hd)] = jnp.broadcast_to(before_log, (8, HEAD))

    with scope("w_relay_0"):
        gated[0].wait_recv()
        gated[6].start()
    with scope("w_filters"):
        for copy in filters:
            copy.wait()
    for hd in (0, 1):
        with scope("w_z"):
            for copy in along_z[hd]:
                copy.wait()
        whole = jnp.zeros((128, HEAD), f32)
        before = jnp.zeros((128, HEAD), f32)
        for k in range(4):
            state, log = unpack_state(z_msg.at[k, hd])
            before = jnp.where(k == z, whole, before)
            whole = whole * jnp.exp(log) + state
        chip_in = before * jnp.exp(a_loc[1 - core, 0:1, lanes(hd)]) + s_loc[1 - core, :, lanes(hd)]
        h_in[0, core, :, lanes(hd)] = chip_in
        h_in[1, core, :, lanes(hd)] = (
            chip_in * jnp.exp(a_loc[core, 0:1, lanes(hd)]) + s_loc[core, :, lanes(hd)]
        )
    swap.start()
    with scope("w_relay_1"):
        gated[1].wait_recv()
        gated[7].start()

    with scope("w_swap"):
        swap.wait()

    with scope("h_units"):
        state = jnp.concatenate([h_in[core, 0], h_in[core, 1]], axis=1)
        for u in range(8):
            h_unit[u] = state.astype(bf16)
            if u < 7:
                state = state * jnp.exp(a_unit[u, 0:1, :]) + s_unit[u]

    def finish_rec(o, k):
        unit = 2 * around(x, o) + k
        rows = slice(k * UNIT, k * UNIT + UNIT)
        for h in range(4):
            rec = near[unit, :, lanes(h)] + lax.dot_general(
                qfar[unit, :, lanes(h)],
                h_unit[unit, :, lanes(h)],
                NT,
                preferred_element_type=f32,
            )
            power = jnp.mean(rec * rec, axis=1, keepdims=True)
            gate = rgate[unit, :, lanes(h)].astype(f32)
            rec = rec * lax.rsqrt(power + head_epsilon) * head_gain[...]
            act[o, rows, lanes(h)] = (rec * (gate * jax.nn.sigmoid(gate))).astype(bf16)

    with scope("fin_rec"):
        finish_rec(2, 0)
        acts[0].start()
        finish_rec(2, 1)
        acts[1].start()
        finish_rec(1, 0)
        acts[2].start()
        finish_rec(3, 0)
        acts[4].start()
        finish_rec(1, 1)
        acts[3].start()
        finish_rec(3, 1)
        acts[5].start()
        finish_rec(0, 0)
        finish_rec(0, 1)

    with scope("w_w5"):
        weights_5()
    def add_product(source, k, p, begin):
        for c in range(4):
            cols = slice(c * 512, c * 512 + 512)
            product = dot(source, w_rel[k, p, :, cols])
            acc[:, cols] = product if begin else acc[:, cols] + product

    with scope("w_gated_1"):
        gated[4].wait_recv()
        gated[5].wait_recv()
    with scope("conv_1"):
        widen(1, 32, 256)
        filter_rows(1, 1)
    with scope("w_gated_3"):
        gated[2].wait_recv()
        gated[3].wait_recv()
    with scope("conv_3"):
        widen(3, 32, 256)
        filter_rows(3, 1)
    with scope("w_edges"):
        for copy in edges:
            copy.wait_recv()
    with scope("conv_13"):
        widen(1, 0, 32)
        filter_rows(1, 0)
        widen(3, 0, 32)
        filter_rows(3, 0)
    with scope("w_gated_2"):
        gated[6].wait_recv()
        gated[7].wait_recv()
    with scope("conv_2"):
        widen(2, 0, 288)
        filter_rows(2, 0)
        filter_rows(2, 1)
    with scope("w_relay_rec"):
        acts[0].wait_recv()
        acts[6].start()
        acts[1].wait_recv()
        acts[7].start()
    with scope("fin_conv"):
        for u in range(2):
            for row in range(0, UNIT, 32):
                rows = slice(row, row + 32)
                wide = filt[u, rows, :]
                mean = jnp.mean(wide, axis=1, keepdims=True)
                centred = wide - mean
                scale = lax.rsqrt(jnp.mean(centred * centred, axis=1, keepdims=True) + norm_epsilon)
                for k in range(4):
                    conv = filt[u, rows, k * 512 : k * 512 + 512] - mean
                    conv = conv * scale * tg[k, 31:32, :]
                    c_act[k, u * UNIT + row : u * UNIT + row + 32, :] = (
                        conv * jax.nn.sigmoid(conv)
                    ).astype(bf16)
    with scope("w_twin"):
        loads[13].wait()
        loads[14].wait()
        for p in (1, 0):
            for n in range(4):
                twin_in[p][n].wait_recv()
    with scope("dot_conv"):
        for k in range(4):
            add_product(c_act[k], k, 1, k == 0)
        add_product(act[0], 0, 0, False)
    with scope("dot_rec"):
        acts[2].wait_recv()
        acts[3].wait_recv()
        add_product(act_in[3], 3, 0, False)
        acts[4].wait_recv()
        acts[5].wait_recv()
        add_product(act_in[1], 1, 0, False)
    with scope("w_rec2"):
        acts[6].wait_recv()
        acts[7].wait_recv()
    with scope("dot_last"):
        for c in range(4):
            cols = slice(c * 512, c * 512 + 512)
            product = dot(act_in[2], w_rel[2, 0, :, cols])
            out[:, cols] = (acc[:, cols] + product).astype(bf16)

    with scope("w_sends"):
        edge.wait_send()
        for copy in gather[0] + gather[1] + cross_out + plane_out[0] + plane_out[1]:
            copy.wait_send()
        for copy in twin_out[0] + twin_out[1] + gated + edges + acts:
            copy.wait_send()


def on_device(
    tokens,
    norm_gain,
    w_query,
    w_forget,
    w_value,
    w_rgate,
    w_glu_value,
    w_glu_gate,
    forget_gap,
    decay_shift,
    head_gain,
    conv_taps,
    conv_gain,
    out_rec,
    out_conv,
):
    vmem = pl.BlockSpec(memory_space=pltpu.VMEM)
    hbm = pl.BlockSpec(memory_space=pl.ANY)
    dma = pltpu.SemaphoreType.DMA
    scratch = [
        pltpu.VMEM((1, 2048), f32),
        pltpu.VMEM((1, 512), f32),
        pltpu.VMEM((4, 1024), f32),
        pltpu.VMEM((1, 128), f32),
        pltpu.VMEM((31, 512), f32),
        pltpu.VMEM((1, 512), f32),
        pltpu.VMEM((256, 2048), bf16),
        pltpu.VMEM((8, 128, 2048), bf16),
        pltpu.VMEM((256, 2048), bf16),
        pltpu.VMEM((6, 2048, 512), bf16),
        pltpu.VMEM((4, 2, 512, 2048), bf16),
        pltpu.VMEM((6, 256, 512), bf16),
        pltpu.VMEM((2, 384, 512), bf16),
        pltpu.VMEM((2, 128, 512), f32),
        pltpu.VMEM((2, 128, 512), f32),
        pltpu.VMEM((2, 128, 512), bf16),
        pltpu.VMEM((8, 128, 512), f32),
        pltpu.VMEM((8, 128, 512), bf16),
        pltpu.VMEM((8, 128, 512), bf16),
        pltpu.VMEM((2, 128, 2048), f32),
        pltpu.VMEM((8, 128, 512), f32),
        pltpu.VMEM((8, 8, 512), f32),
        pltpu.VMEM((8, 128, 512), bf16),
        pltpu.VMEM((2, 128, 256), f32),
        pltpu.VMEM((2, 8, 256), f32),
        pltpu.VMEM((144, 256), bf16),
        pltpu.VMEM((144, 256), bf16),
        pltpu.VMEM((4, 2, 144, 128), bf16),
        pltpu.VMEM((4, 2, 144, 128), bf16),
        pltpu.VMEM((2, 2, 128, 256), f32),
        pltpu.VMEM((4, 256, 512), bf16),
        pltpu.VMEM((4, 256, 512), bf16),
        pltpu.VMEM((2, 2, 128, 512), bf16),
        pltpu.VMEM((256, 2048), f32),
        pltpu.VMEM((2, 16, 2048), bf16),
        pltpu.VMEM((1056, 512), bf16),
        pltpu.VMEM((4, 288, 512), bf16),
        pltpu.VMEM((16, 288, 128), f32),
        pltpu.VMEM((4, 256, 512), bf16),
        pltpu.VMEM((4, 32, 512), f32),
        dma((17,)),
        dma((2, 7)),
        dma((2, 7)),
        dma((15,)),
        dma((15,)),
        dma((4,)),
        dma((4,)),
        dma((6,)),
        dma((6,)),
        dma((2, 20)),
        dma((2, 20)),
        dma((2, 4)),
        dma((2, 4)),
        dma((2, 11)),
        dma((2, 11)),
    ]
    return pl.pallas_call(
        kernel,
        out_shape=pltpu.VMEM((256, 2048), bf16),
        in_specs=[hbm] * 15,
        out_specs=vmem,
        scratch_shapes=scratch,
        compiler_params=pltpu.CompilerParams(
            collective_id=0, has_side_effects=True, vmem_limit_bytes=60 * 1024 * 1024
        ),
    )(
        tokens,
        norm_gain[None],
        w_query,
        w_forget,
        w_value,
        w_rgate,
        w_glu_value,
        w_glu_gate,
        forget_gap[None],
        decay_shift.T,
        head_gain[None],
        conv_taps,
        conv_gain[None],
        out_rec,
        out_conv,
    )


def solution(mesh):
    placed = (
        P(("sp", "tp"), None),
        P(),
        P(None, "tp"),
        P(None, "tp"),
        P(None, "tp"),
        P(None, "tp"),
        P(None, "tp"),
        P(None, "tp"),
        P("tp"),
        P("sp", "tp"),
        P(),
        P(None, "tp"),
        P("tp"),
        P("tp", None),
        P("tp", None),
    )
    return jax.shard_map(
        on_device, mesh=mesh, in_specs=placed, out_specs=P(("sp", "tp"), None), check_vma=False
    )
```

time: 94 us -> 81.9 us (0.87)
  Pallas kernels: 91.6 us -> 80.2 us
  local copies, waits for them, and re-layouts: 2.3 us -> 0.97 us
    pallas_call x1, Pallas kernels: 91.6 us -> 80.2 us  [on_device(): pl.pallas_call(kernel, out_shape=pltpu.VMEM((256, 2048), bf16), in_specs=...]
    unnamed x1, local copies, waits for them, and re-layouts: 2.3 us -> 0.97 us
where the time goes in v3:
time: 81.9 us; the launch traced here: 81.2 us
  Pallas kernels  80.2 us (98%)
  local copies, waits for them, and re-layouts  0.97 us (1%)
    pallas_call x1, Pallas kernels, on_device(): pl.pallas_call(kernel, out_shape=pltpu.VMEM((256, 2048), bf16), in_specs=...  80.2 us

profile of v3, /device:TPU:0, one launch (start us, length us, event | category | flops | bytes accessed | tf_op | source)
XLA Modules:
  0.0 81.2 jit_solution(12389827266132975195)
XLA Ops:
  0.0 80.2 %shard_map.145 = bf16[256,2048]{1,0:T(8,128)(2,1)S(1)} custom-call(bf16[256,2048]{1,0:T(8,128)(2,1)} %tokens.1, f32[1,2048]{1,0:T(1,128)} %bitcast.6, bf16[2048,512]{1,0:T(8,128)(2,1)} %w_query.1, bf16[2048,512]{1,0:T(8,128)(2,1)} %w_forget.1, bf16[2048,512]{1,0:T(8,128)(2,1)} %w_value.1, bf16[2048,512]{1,0:T(8,128)(2,1)} %w_rgate.1, ...), custom_call_target="tpu_custom_call" | custom-call | tf_op jit(solution)/shard_map/pallas_call | solution.py:926
  80.2 1.0 %copy.17 = bf16[256,2048]{1,0:T(8,128)(2,1)} copy(bf16[256,2048]{1,0:T(8,128)(2,1)S(1)} %shard_map.145) | data formatting | bytes 2097152

commit v4 on v3

--- a/solution.py
+++ b/solution.py
@@ -105,21 +105,7 @@
     c_pad,
     c_act,
     tg,
-    load_sem,
-    ag_send,
-    ag_recv,
-    sp_send,
-    sp_recv,
-    st_send,
-    st_recv,
-    wx_send,
-    wx_recv,
-    wp_send,
-    wp_recv,
-    wc_send,
-    wc_recv,
-    aa_send,
-    aa_recv,
+    sems,
 ):
     x = lax.axis_index("tp")
     s = lax.axis_index("sp")
@@ -167,8 +153,11 @@
     own_rows = [slice_rows(p, first_index[p], second_index[p]) for p in (0, 1)]
     weight_of = (out_rec, out_conv)
 
+    def wait_for(ref, k):
+        pltpu.make_async_copy(ref, ref, sems.at[k]).wait()
+
     own_loads = [
-        pltpu.make_async_copy(weight_of[p].at[own_rows[p]], w_own.at[p], load_sem.at[15 + p])
+        pltpu.make_async_copy(weight_of[p].at[own_rows[p]], w_own.at[p], sems.at[9])
         for p in (0, 1)
     ]
     pairs = [(tokens, tok), (norm_gain_hbm, norm_gain)]
@@ -188,14 +177,16 @@
         (out_conv, w_rel.at[0, 1]),
     ]
     loads = [
-        pltpu.make_async_copy(src, dst, load_sem.at[k]) for k, (src, dst) in enumerate(pairs)
+        pltpu.make_async_copy(src, dst, sems.at[(0, 1, 2, 2, 2, 2, 2, 2, 3, 4, 5, 6, 7, 8, 8)[k]])
+        for k, (src, dst) in enumerate(pairs)
     ]
     for load in own_loads + loads:
         load.start()
 
     def cross(k, p, slot, src, target):
         dst = w_rel.at[slot, p, own_rows[p]]
-        return remote(src, dst, wx_send.at[k], wx_recv.at[k], {"tp": target})
+        come = (17, 19, 19, 18, 19, 19)[k]
+        return remote(src, dst, sems.at[16], sems.at[come], {"tp": target})
 
     def own_slice(p):
         return w_own.at[p]
@@ -208,7 +199,6 @@
         cross(4, 0, 2, w_rel.at[3, 0, own_rows[0]], right),
         cross(5, 1, 2, w_rel.at[1, 1, own_rows[1]], left),
     ]
-    cross_in = cross_out
 
     def packet(p, j1, j2, half):
         cols = pl.ds(0, 2048) if half is None else pl.ds(1024 * half, 1024)
@@ -216,9 +206,10 @@
 
     def plane(p, k, j1, j2, half, target):
         ref = packet(p, j1, j2, half)
-        return remote(ref, ref, wp_send.at[p, k], wp_recv.at[p, k], {"sp": target})
-
-    plane_out, plane_in = [], []
+        return remote(ref, ref, sems.at[20], sems.at[plane_sem[k]], {"sp": target})
+
+    plane_sem = (21, 21, 22, 22, 23, 23, 26, 26, 24, 24, 26, 26, 25, 25, 26, 26, 24, 24, 26, 26)
+    plane_out = []
     for p in (0, 1):
         i1, i2 = first_index[p], second_index[p]
         to1, to2 = first_at[p], second_at[p]
@@ -228,12 +219,6 @@
             (around(i1, 3), i2, 0, to1(1)),
             (around(i1, 1), i2, 1, to1(3)),
         ]
-        comes = [
-            (around(i1, 3), i2, None),
-            (around(i1, 1), i2, None),
-            (around(i1, 2), i2, 0),
-            (around(i1, 2), i2, 1),
-        ]
         for m in range(4):
             j1 = around(i1, m)
             sends += [
@@ -242,29 +227,18 @@
                 (j1, around(i2, 3), 0, to2(1)),
                 (j1, around(i2, 1), 1, to2(3)),
             ]
-            comes += [
-                (j1, around(i2, 3), None),
-                (j1, around(i2, 1), None),
-                (j1, around(i2, 2), 0),
-                (j1, around(i2, 2), 1),
-            ]
         plane_out.append([plane(p, k, *send) for k, send in enumerate(sends)])
-        plane_in.append(
-            [plane(p, k, *come, sends[k][3]) for k, come in enumerate(comes)]
-        )
 
     def twin(p, n, owner):
         j2 = around(second_index[p], (0, 3, 1, 2)[n])
         rows = pl.ds(pl.multiple_of(256 * owner + 64 * j2, 64), 64)
         ref = w_rel.at[pl.ds(1, 3), p, rows]
-        return remote(ref, ref, wc_send.at[p, n], wc_recv.at[p, n], {"sp": partner})
+        return remote(ref, ref, sems.at[27], sems.at[28], {"sp": partner})
 
     twin_out = [[twin(p, n, core) for n in range(4)] for p in (0, 1)]
-    twin_in = [[twin(p, n, 1 - core) for n in range(4)] for p in (0, 1)]
-
-    def receive(k):
-        for p in (1, 0):
-            plane_in[p][k].wait_recv()
+
+    def receive(k, rows):
+        wait_for(w_rel.at[pl.ds(1, 3), 0, pl.ds(0, rows)], k)
 
     def start(*ks):
         for k in ks:
@@ -272,37 +246,35 @@
                 plane_out[p][k].start()
 
     def weights_0():
-        for k in (1, 2, 4, 5):
-            cross_in[k].wait_recv()
+        wait_for(xn.at[0, pl.ds(0, 64)], 19)
         start(0, 1, 4, 5)
 
     def weights_1():
-        receive(0)
-        receive(1)
+        receive(21, 64)
         start(2, 3)
         start(16, 17, 8, 9)
 
     def weights_2():
-        receive(2)
-        receive(3)
+        receive(22, 32)
         start(12, 13)
         for p in (1, 0):
             twin_out[p][0].start()
-
-    def weights_3(m):
-        receive(4 + 4 * m)
-        receive(5 + 4 * m)
-        start(6 + 4 * m, 7 + 4 * m)
+        receive(23, 64)
+        start(6, 7)
+
+    def weights_3():
+        receive(24, 128)
+        start(18, 19, 10, 11)
 
     def weights_4():
+        receive(25, 64)
+        start(14, 15)
         for p in (1, 0):
             twin_out[p][1].start()
             twin_out[p][2].start()
 
     def weights_5():
-        for m in (0, 3, 1, 2):
-            receive(6 + 4 * m)
-            receive(7 + 4 * m)
+        receive(26, 128)
         for p in (1, 0):
             twin_out[p][3].start()
 
@@ -318,13 +290,13 @@
     def rows_copy(unit, begin, size, k, way):
         ref = xn.at[unit, pl.ds(begin, size)]
         target = {"tp": left if way else right}
-        return remote(ref, ref, ag_send.at[way, k], ag_recv.at[way, k], target)
+        return remote(ref, ref, sems.at[10], sems.at[(11, 11, 11, 12, 13, 14, 15)[k]], target)
 
     parts = (
         ((1, 0, 32), (1, 32, 32), (1, 64, 64), (0, 0, 64), (0, 64, 64), (0, 0, 64), (1, 0, 64)),
         ((0, 64, 32), (0, 96, 32), (0, 0, 64), (1, 64, 64), (1, 0, 64), (0, 64, 64), (1, 64, 64)),
     )
-    gather, arrive = [], []
+    gather = []
     for way in (0, 1):
         source = left if way == 0 else right
         gather.append(
@@ -333,35 +305,27 @@
                 for k, (u, begin, size) in enumerate(parts[way])
             ]
         )
-        arrive.append(
-            [
-                rows_copy(2 * (source if k < 5 else far) + u, begin, size, k, way)
-                for k, (u, begin, size) in enumerate(parts[way])
-            ]
-        )
-
-    def tokens_in(*ks):
-        for k in ks:
-            arrive[0][k].wait_recv()
-            arrive[1][k].wait_recv()
-
-    loads[0].wait()
-    loads[1].wait()
+
+    def tokens_in(k):
+        wait_for(xn.at[pl.ds(0, 2)] if k == 0 else xn.at[0], (11, None, None, 12, 13, 14, 15)[k])
+
+    wait_for(w_own, 9)
+    with scope("w_barrier"):
+        pl.semaphore_wait(barrier, len(peers))
+    for k in range(4):
+        cross_out[k].start()
+    with scope("w_tok"):
+        loads[0].wait()
+        loads[1].wait()
     with scope("ln"):
         norm_rows(0)
         norm_rows(1)
-    with scope("w_barrier"):
-        pl.semaphore_wait(barrier, len(peers))
-    for load in own_loads:
-        load.wait()
-    for k in range(4):
-        cross_out[k].start()
     gather[0][0].start()
     gather[1][0].start()
     with scope("w_cross"):
-        cross_in[0].wait_recv()
+        cross_out[0].wait_recv()
         cross_out[4].start()
-        cross_in[3].wait_recv()
+        cross_out[3].wait_recv()
         cross_out[5].start()
     for k in range(1, 5):
         gather[0][k].start()
@@ -434,10 +398,10 @@
             near[unit, :, lanes(h)] = dot(scores, raw[1, rows, lanes(h)])
             rgate[unit, :, lanes(h)] = raw[3, rows, lanes(h)]
 
-    def sp_copy(src, dst, k, target):
-        return remote(src, dst, sp_send.at[k], sp_recv.at[k], {"sp": target})
-
-    edge = sp_copy(mixed_in.at[pl.ds(1024, 32)], mixed_in.at[pl.ds(0, 32)], 1, ahead)
+    def sp_copy(ref, dst, send, come, target):
+        return remote(ref, dst, sems.at[send], sems.at[come], {"sp": target})
+
+    edge = sp_copy(mixed_in.at[pl.ds(1024, 32)], mixed_in.at[pl.ds(0, 32)], 31, 32, ahead)
 
     def send_edge(owner):
         @pl.when(x == owner)
@@ -448,7 +412,9 @@
         return mixed_in.at[pl.ds(pl.multiple_of(256 * around(x, o) + begin, 32), size)]
 
     def hop(p, k, src, dst, target):
-        return remote(src, dst, aa_send.at[p, k], aa_recv.at[p, k], {"tp": target})
+        send = (52, 44, 50)[p]
+        come = 51 if p == 2 else (53, 45)[p] + (0, 1, 2, 2, 3, 3, 4, 4)[k]
+        return remote(src, dst, sems.at[send], sems.at[come], {"tp": target})
 
     low, high = pl.ds(0, UNIT), pl.ds(UNIT, UNIT)
     low_in, high_in = pl.ds(32, UNIT), pl.ds(32 + UNIT, UNIT)
@@ -463,7 +429,7 @@
         hop(1, 7, relay.at[1, 1], c_in.at[2, high_in], right),
     ]
     edges = [
-        hop(1, 7 + o, rows_of(o, 0, 32), c_in.at[4 - o, pl.ds(0, 32)], {1: right, 2: far, 3: left}[o])
+        hop(2, o, rows_of(o, 0, 32), c_in.at[4 - o, pl.ds(0, 32)], {1: right, 2: far, 3: left}[o])
         for o in (1, 2, 3)
     ]
     acts = [
@@ -477,7 +443,7 @@
         hop(0, 7, relay.at[0, 1], act_in.at[2, high], right),
     ]
     filters = [
-        remote(tg.at[0], tg.at[4 - j], st_send.at[j], st_recv.at[j], {"tp": around(x, j)})
+        remote(tg.at[0], tg.at[4 - j], sems.at[42], sems.at[43], {"tp": around(x, j)})
         for j in (1, 2, 3)
     ]
 
@@ -488,7 +454,8 @@
         @pl.when(step == 0)
         def _():
             with scope("w_weights"):
-                for k in range(2, 13):
+                wait_for(w_in, 2)
+                for k in range(8, 13):
                     loads[k].wait()
             tg[0, 0:31, :] = taps[...]
             tg[0, 31:32, :] = conv_gain[...]
@@ -496,9 +463,8 @@
         @pl.when(step == 1)
         def _():
             with scope("w_ag1"):
-                tokens_in(0, 1)
+                tokens_in(0)
                 gather[1][5].start()
-                tokens_in(2)
 
         @pl.when(step == 2)
         def _():
@@ -512,7 +478,6 @@
                 tokens_in(4)
             with scope("w_w2"):
                 weights_2()
-                weights_3(0)
 
         with scope("proj_fv"):
             xp[0:UNIT, :] = xn[unit_a]
@@ -558,8 +523,7 @@
             raw[k, 0:UNIT, :] = dot(xn[unit], w_in[k]).astype(bf16)
 
     with scope("w_w3_31"):
-        weights_3(3)
-        weights_3(1)
+        weights_3()
     with scope("w_far_a"):
         tokens_in(5)
     with scope("far_a"):
@@ -574,16 +538,19 @@
         project_unit(2 * far + 1, 0, 1)
         gates(0, 2 * far + 1, unit_rows)
 
-    pair = sp_copy(p_send, p_recv, 0, partner)
+    pair = sp_copy(p_send, p_recv, 29, 30, partner)
     along_y = [
-        [sp_copy(y_msg.at[y, hd], y_msg.at[y, hd], 1 + 3 * hd + k, at_y(k)) for k in (2, 1, 3)]
+        [sp_copy(y_msg.at[y, hd], y_msg.at[y, hd], 33, 34 + hd, at_y(k)) for k in (2, 1, 3)]
         for hd in (0, 1)
     ]
     along_z = [
-        [sp_copy(z_msg.at[z, hd], z_msg.at[z, hd], 7 + 3 * hd + k, at_z(k)) for k in (2, 1, 3)]
+        [sp_copy(z_msg.at[z, hd], z_msg.at[z, hd], 36, 37 + hd, at_z(k)) for k in (2, 1, 3)]
         for hd in (0, 1)
     ]
-    swap = sp_copy(h_in.at[1 - core, core], h_in.at[1 - core, core], 14, partner)
+    swap = [
+        sp_copy(h_in.at[1 - core, core, hd], h_in.at[1 - core, core, hd], 39, 40 + hd, partner)
+        for hd in (0, 1)
+    ]
 
     with scope("combine"):
         state = s_unit[0]
@@ -601,7 +568,7 @@
         p_send[128:144, :] = extra
         pair.start()
     with scope("w_pair"):
-        pair.wait()
+        pair.wait_recv()
     mine, mine_log = s_loc[core], a_loc[core, 0:1, :]
     other, other_log = unpack_state(p_recv)
     first = jnp.where(core == 0, mine, other)
@@ -629,7 +596,6 @@
         gated[3].start()
 
     with scope("w_w3_2"):
-        weights_3(2)
         weights_4()
 
     with scope("proj_qr"):
@@ -671,8 +637,7 @@
 
     for hd in (0, 1):
         with scope("w_y"):
-            for copy in along_y[hd]:
-                copy.wait()
+            wait_for(y_msg.at[pl.ds(0, 3), hd], 34 + hd)
         whole = jnp.zeros((128, HEAD), f32)
         whole_log = jnp.zeros((1, HEAD), f32)
         before = jnp.zeros((128, HEAD), f32)
@@ -695,12 +660,10 @@
         gated[0].wait_recv()
         gated[6].start()
     with scope("w_filters"):
-        for copy in filters:
-            copy.wait()
+        wait_for(tg.at[pl.ds(0, 3)], 43)
     for hd in (0, 1):
         with scope("w_z"):
-            for copy in along_z[hd]:
-                copy.wait()
+            wait_for(z_msg.at[pl.ds(0, 3), hd], 37 + hd)
         whole = jnp.zeros((128, HEAD), f32)
         before = jnp.zeros((128, HEAD), f32)
         for k in range(4):
@@ -708,20 +671,21 @@
             before = jnp.where(k == z, whole, before)
             whole = whole * jnp.exp(log) + state
         chip_in = before * jnp.exp(a_loc[1 - core, 0:1, lanes(hd)]) + s_loc[1 - core, :, lanes(hd)]
-        h_in[0, core, :, lanes(hd)] = chip_in
-        h_in[1, core, :, lanes(hd)] = (
+        h_in[0, core, hd] = chip_in.astype(bf16)
+        h_in[1, core, hd] = (
             chip_in * jnp.exp(a_loc[core, 0:1, lanes(hd)]) + s_loc[core, :, lanes(hd)]
-        )
-    swap.start()
+        ).astype(bf16)
+        swap[hd].start()
     with scope("w_relay_1"):
         gated[1].wait_recv()
         gated[7].start()
 
     with scope("w_swap"):
-        swap.wait()
+        swap[0].wait_recv()
+        swap[1].wait_recv()
 
     with scope("h_units"):
-        state = jnp.concatenate([h_in[core, 0], h_in[core, 1]], axis=1)
+        state = jnp.concatenate([h_in[core, h // 2, h % 2].astype(f32) for h in range(4)], axis=1)
         for u in range(8):
             h_unit[u] = state.astype(bf16)
             if u < 7:
@@ -767,28 +731,24 @@
             acc[:, cols] = product if begin else acc[:, cols] + product
 
     with scope("w_gated_1"):
-        gated[4].wait_recv()
-        gated[5].wait_recv()
+        wait_for(c_in.at[1, pl.ds(32, 256)], 48)
     with scope("conv_1"):
         widen(1, 32, 256)
         filter_rows(1, 1)
     with scope("w_gated_3"):
-        gated[2].wait_recv()
-        gated[3].wait_recv()
+        wait_for(c_in.at[3, pl.ds(32, 256)], 47)
     with scope("conv_3"):
         widen(3, 32, 256)
         filter_rows(3, 1)
     with scope("w_edges"):
-        for copy in edges:
-            copy.wait_recv()
+        wait_for(mixed_in.at[pl.ds(0, 96)], 51)
     with scope("conv_13"):
         widen(1, 0, 32)
         filter_rows(1, 0)
         widen(3, 0, 32)
         filter_rows(3, 0)
     with scope("w_gated_2"):
-        gated[6].wait_recv()
-        gated[7].wait_recv()
+        wait_for(c_in.at[2, pl.ds(32, 256)], 49)
     with scope("conv_2"):
         widen(2, 0, 288)
         filter_rows(2, 0)
@@ -813,25 +773,19 @@
                         conv * jax.nn.sigmoid(conv)
                     ).astype(bf16)
     with scope("w_twin"):
-        loads[13].wait()
-        loads[14].wait()
-        for p in (1, 0):
-            for n in range(4):
-                twin_in[p][n].wait_recv()
+        wait_for(w_rel.at[0], 8)
+        wait_for(w_rel.at[pl.ds(1, 3), 0], 28)
     with scope("dot_conv"):
         for k in range(4):
             add_product(c_act[k], k, 1, k == 0)
         add_product(act[0], 0, 0, False)
     with scope("dot_rec"):
-        acts[2].wait_recv()
-        acts[3].wait_recv()
+        wait_for(act_in.at[3], 55)
         add_product(act_in[3], 3, 0, False)
-        acts[4].wait_recv()
-        acts[5].wait_recv()
+        wait_for(act_in.at[1], 56)
         add_product(act_in[1], 1, 0, False)
     with scope("w_rec2"):
-        acts[6].wait_recv()
-        acts[7].wait_recv()
+        wait_for(act_in.at[2], 57)
     with scope("dot_last"):
         for c in range(4):
             cols = slice(c * 512, c * 512 + 512)
@@ -840,10 +794,18 @@
 
     with scope("w_sends"):
         edge.wait_send()
-        for copy in gather[0] + gather[1] + cross_out + plane_out[0] + plane_out[1]:
-            copy.wait_send()
-        for copy in twin_out[0] + twin_out[1] + gated + edges + acts:
-            copy.wait_send()
+        pair.wait_send()
+        wait_for(xn.at[pl.ds(0, 6)], 10)
+        wait_for(xn.at[0, pl.ds(0, 96)], 16)
+        wait_for(w_rel.at[pl.ds(1, 3), 0, pl.ds(0, 480)], 20)
+        wait_for(w_rel.at[pl.ds(1, 3), 0], 27)
+        wait_for(y_msg.at[pl.ds(0, 3)], 33)
+        wait_for(z_msg.at[pl.ds(0, 3)], 36)
+        wait_for(h_in.at[0, 0], 39)
+        wait_for(tg.at[pl.ds(0, 3)], 42)
+        wait_for(act, 44)
+        wait_for(mixed_in.at[pl.ds(0, 96)], 50)
+        wait_for(act, 52)
 
 
 def on_device(
@@ -896,7 +858,7 @@
         pltpu.VMEM((144, 256), bf16),
         pltpu.VMEM((4, 2, 144, 128), bf16),
         pltpu.VMEM((4, 2, 144, 128), bf16),
-        pltpu.VMEM((2, 2, 128, 256), f32),
+        pltpu.VMEM((2, 2, 2, 128, 128), bf16),
         pltpu.VMEM((4, 256, 512), bf16),
         pltpu.VMEM((4, 256, 512), bf16),
         pltpu.VMEM((2, 2, 128, 512), bf16),
@@ -907,21 +869,7 @@
         pltpu.VMEM((16, 288, 128), f32),
         pltpu.VMEM((4, 256, 512), bf16),
         pltpu.VMEM((4, 32, 512), f32),
-        dma((17,)),
-        dma((2, 7)),
-        dma((2, 7)),
-        dma((15,)),
-        dma((15,)),
-        dma((4,)),
-        dma((4,)),
-        dma((6,)),
-        dma((6,)),
-        dma((2, 20)),
-        dma((2, 20)),
-        dma((2, 4)),
-        dma((2, 4)),
-        dma((2, 11)),
-        dma((2, 11)),
+        dma((58,)),
     ]
     return pl.pallas_call(
         kernel,

time: 81.9 us -> 79.8 us (0.974)
  Pallas kernels: 80.2 us -> 78.3 us
    pallas_call x1, Pallas kernels: 80.2 us -> 78.3 us  [on_device(): pl.pallas_call(kernel, out_shape=pltpu.VMEM((256, 2048), bf16), in_specs=...]
where the time goes in v4:
time: 79.8 us; the launch traced here: 79.3 us
  Pallas kernels  78.3 us (98%)
  local copies, waits for them, and re-layouts  0.97 us (1%)
    pallas_call x1, Pallas kernels, on_device(): pl.pallas_call(kernel, out_shape=pltpu.VMEM((256, 2048), bf16), in_specs=...  78.3 us

profile of v4, /device:TPU:0, one launch (start us, length us, event | category | flops | bytes accessed | tf_op | source)
XLA Modules:
  0.0 79.3 jit_solution(11958468150729585953)
XLA Ops:
  0.0 78.3 %shard_map.145 = bf16[256,2048]{1,0:T(8,128)(2,1)S(1)} custom-call(bf16[256,2048]{1,0:T(8,128)(2,1)} %tokens.1, f32[1,2048]{1,0:T(1,128)} %bitcast.6, bf16[2048,512]{1,0:T(8,128)(2,1)} %w_query.1, bf16[2048,512]{1,0:T(8,128)(2,1)} %w_forget.1, bf16[2048,512]{1,0:T(8,128)(2,1)} %w_value.1, bf16[2048,512]{1,0:T(8,128)(2,1)} %w_rgate.1, ...), custom_call_target="tpu_custom_call" | custom-call | tf_op jit(solution)/shard_map/pallas_call | solution.py:874
  78.3 1.0 %copy.17 = bf16[256,2048]{1,0:T(8,128)(2,1)} copy(bf16[256,2048]{1,0:T(8,128)(2,1)S(1)} %shard_map.145) | data formatting | bytes 2097152

commit v5 on v4

--- a/solution.py
+++ b/solution.py
@@ -473,8 +473,6 @@
                 gather[0][5].start()
                 gather[0][6].start()
                 gather[1][6].start()
-                for copy in filters:
-                    copy.start()
                 tokens_in(4)
             with scope("w_w2"):
                 weights_2()
@@ -534,6 +532,10 @@
         scan(0, 2 * far, unit_rows)
     with scope("w_far_b"):
         tokens_in(6)
+    for copy in filters:
+        copy.start()
+    for k in (0, 2, 5, 4):
+        gated[k].start()
     with scope("far_b"):
         project_unit(2 * far + 1, 0, 1)
         gates(0, 2 * far + 1, unit_rows)
@@ -586,8 +588,6 @@
         for copy in along_y[hd]:
             copy.start()
 
-    for k in (0, 2, 4, 5):
-        gated[k].start()
     with scope("proj_glu"):
         project_unit(2 * far + 1, 4, 5)
         mix(0, 2 * far + 1, unit_rows)
@@ -620,20 +620,6 @@
                     + tg[k, j : j + 1, lanes(g)] * c_pad[4 * k + g, begin : begin + UNIT, :]
                 )
             filt[u, :, lanes(4 * k + g)] = total
-
-    with scope("w_edge"):
-        edge.wait_recv()
-
-        @pl.when(s == 0)
-        def _():
-            mixed_in[0:32, :] = jnp.zeros((32, 512), bf16)
-
-    for copy in edges:
-        copy.start()
-    with scope("conv_0"):
-        widen(0, 0, 288)
-        filter_rows(0, 0)
-        filter_rows(0, 1)
 
     for hd in (0, 1):
         with scope("w_y"):
@@ -659,6 +645,20 @@
     with scope("w_relay_0"):
         gated[0].wait_recv()
         gated[6].start()
+    with scope("w_edge"):
+        edge.wait_recv()
+
+        @pl.when(s == 0)
+        def _():
+            mixed_in[0:32, :] = jnp.zeros((32, 512), bf16)
+
+    for copy in edges:
+        copy.start()
+    with scope("conv_0"):
+        widen(0, 0, 288)
+        filter_rows(0, 0)
+        filter_rows(0, 1)
+
     with scope("w_filters"):
         wait_for(tg.at[pl.ds(0, 3)], 43)
     for hd in (0, 1):
@@ -676,9 +676,10 @@
             chip_in * jnp.exp(a_loc[core, 0:1, lanes(hd)]) + s_loc[core, :, lanes(hd)]
         ).astype(bf16)
         swap[hd].start()
-    with scope("w_relay_1"):
-        gated[1].wait_recv()
-        gated[7].start()
+        if hd == 0:
+            with scope("w_relay_1"):
+                gated[1].wait_recv()
+                gated[7].start()
 
     with scope("w_swap"):
         swap[0].wait_recv()

time: 79.8 us -> 77.5 us (0.971)
  Pallas kernels: 78.3 us -> 75.7 us
    pallas_call x1, Pallas kernels: 78.3 us -> 75.7 us  [on_device(): pl.pallas_call(kernel, out_shape=pltpu.VMEM((256, 2048), bf16), in_specs=...]
where the time goes in v5:
time: 77.5 us; the launch traced here: 76.7 us
  Pallas kernels  75.7 us (98%)
  local copies, waits for them, and re-layouts  0.97 us (1%)
    pallas_call x1, Pallas kernels, on_device(): pl.pallas_call(kernel, out_shape=pltpu.VMEM((256, 2048), bf16), in_specs=...  75.7 us

profile of v5, /device:TPU:0, one launch (start us, length us, event | category | flops | bytes accessed | tf_op | source)
XLA Modules:
  0.0 76.7 jit_solution(10536112731528039332)
XLA Ops:
  0.0 75.7 %shard_map.145 = bf16[256,2048]{1,0:T(8,128)(2,1)S(1)} custom-call(bf16[256,2048]{1,0:T(8,128)(2,1)} %tokens.1, f32[1,2048]{1,0:T(1,128)} %bitcast.6, bf16[2048,512]{1,0:T(8,128)(2,1)} %w_query.1, bf16[2048,512]{1,0:T(8,128)(2,1)} %w_forget.1, bf16[2048,512]{1,0:T(8,128)(2,1)} %w_value.1, bf16[2048,512]{1,0:T(8,128)(2,1)} %w_rgate.1, ...), custom_call_target="tpu_custom_call" | custom-call | tf_op jit(solution)/shard_map/pallas_call | solution.py:875
  75.7 1.0 %copy.17 = bf16[256,2048]{1,0:T(8,128)(2,1)} copy(bf16[256,2048]{1,0:T(8,128)(2,1)S(1)} %shard_map.145) | data formatting | bytes 2097152

commit v6 on v5

--- a/solution.py
+++ b/solution.py
@@ -129,8 +129,8 @@
         return (around(z, k) * 4 + y) * 2 + core
 
     barrier = pltpu.get_barrier_semaphore()
-    peers = [{"tp": right}, {"tp": left}, {"tp": far}, {"sp": partner}, {"sp": behind}]
-    peers += [{"sp": at_y(k)} for k in (1, 2, 3)] + [{"sp": at_z(k)} for k in (1, 2, 3)]
+    peers = [{"tp": right}, {"tp": left}, {"sp": partner}, {"sp": behind}]
+    peers += [{"sp": at_y(k)} for k in (1, 3)] + [{"sp": at_z(k)} for k in (1, 3)]
     for peer in peers:
         pl.semaphore_signal(barrier, inc=1, device_id=peer, device_id_type=MESH)
 

time: 77.5 us -> 77.2 us (level)
  no operation moved by 1% of the time
where the time goes in v6:
time: 77.2 us; the launch traced here: 76.5 us
  Pallas kernels  75.5 us (98%)
  local copies, waits for them, and re-layouts  0.97 us (1%)
    pallas_call x1, Pallas kernels, on_device(): pl.pallas_call(kernel, out_shape=pltpu.VMEM((256, 2048), bf16), in_specs=...  75.5 us

profile of v6, /device:TPU:0, one launch (start us, length us, event | category | flops | bytes accessed | tf_op | source)
XLA Modules:
  0.0 76.5 jit_solution(8502884120900706167)
XLA Ops:
  0.0 75.5 %shard_map.145 = bf16[256,2048]{1,0:T(8,128)(2,1)S(1)} custom-call(bf16[256,2048]{1,0:T(8,128)(2,1)} %tokens.1, f32[1,2048]{1,0:T(1,128)} %bitcast.6, bf16[2048,512]{1,0:T(8,128)(2,1)} %w_query.1, bf16[2048,512]{1,0:T(8,128)(2,1)} %w_forget.1, bf16[2048,512]{1,0:T(8,128)(2,1)} %w_value.1, bf16[2048,512]{1,0:T(8,128)(2,1)} %w_rgate.1, ...), custom_call_target="tpu_custom_call" | custom-call | tf_op jit(solution)/shard_map/pallas_call | solution.py:875
  75.5 1.0 %copy.17 = bf16[256,2048]{1,0:T(8,128)(2,1)} copy(bf16[256,2048]{1,0:T(8,128)(2,1)S(1)} %shard_map.145) | data formatting | bytes 2097152
